TPU v7x, 32 devices: a whole 2x2x4 slice. The times are simulated.
32 devices in a mesh: sp: 8 (over z, y), tp: 4 (over x, core).
Axes of the slice: x: 2, y: 2, z: 4, core: 2. Of those that a mesh axis runs over, the one named last changes fastest.
Arguments:
- stream: bfloat16 [2048, 2048], P('sp'), may hold values from -6 to 6
- attn_gain: float32 [2, 2048], replicated, may hold values from 0.1 to 1.9
- w_query: bfloat16 [2, 2048, 2048], P(None, None, 'tp'), may hold values from -0.125 to 0.125
- w_key: bfloat16 [2, 2048, 512], P(None, None, 'tp'), may hold values from -0.125 to 0.125
- w_value: bfloat16 [2, 2048, 512], P(None, None, 'tp'), may hold values from -0.125 to 0.125
- w_out: bfloat16 [2, 2048, 2048], P(None, 'tp'), may hold values from -1 to 1
- query_gain: float32 [2, 64], replicated, may hold values from 0.1 to 1.9
- key_gain: float32 [2, 64], replicated, may hold values from 0.1 to 1.9
- rel_bias: float32 [2, 32, 257], P(None, 'tp'), may hold values from -6 to 300
Outputs:
- result: bfloat16 [2048, 2048], P('sp', 'tp')
All inputs are finite; a program needn't handle non-finite values.
Results may differ from a plain program's by a relative error of at most 0.02.
Values may be sent and summed in bfloat16 or wider, within the bound.
A program may use at most 64 MiB of HBM per device.

v0:
```python
import functools

import jax
import jax.numpy as jnp
from jax import lax
from jax.experimental import pallas as pl
from jax.experimental.pallas import tpu as pltpu
from jax.sharding import PartitionSpec as P

HEAD_DIM = 64
SEG = 64
LEFT = 4
CLIP = 128
LAYERS = 2
SPAN = (LEFT + 1) * SEG
LINE = 384
SUBS = 2

norm_eps = 1e-06
masked_score = -1e30
F32 = jnp.float32
BF16 = jnp.bfloat16


def seg_rows(seg):
    return pl.ds(pl.multiple_of(seg * SEG, SEG), SEG)


def send(src, dst, send_sem, recv_sem, device):
    return pltpu.make_async_remote_copy(
        src_ref=src,
        dst_ref=dst,
        send_sem=send_sem,
        recv_sem=recv_sem,
        device_id=device,
        device_id_type=pl.DeviceIdType.MESH,
    )


def row_norm(x, gain):
    squared = jnp.mean(x * x, axis=-1, keepdims=True)
    return (x * lax.rsqrt(squared + norm_eps) * gain).astype(BF16)


def head_norm(x, gain_row, scale):
    width = x.shape[1]
    block = min(width, 256)
    row_head = lax.broadcasted_iota(jnp.int32, (block, block), 0) >> 6
    col_head = lax.broadcasted_iota(jnp.int32, (block, block), 1) >> 6
    spread = jnp.where(row_head == col_head, 1.0 / HEAD_DIM, 0.0).astype(BF16)
    gain = jnp.concatenate([gain_row] * (block // HEAD_DIM), axis=1) * scale
    outs = []
    for lower in range(0, width, block):
        part = x[:, lower : lower + block]
        squares = part * part
        high = squares.astype(BF16)
        low = (squares - high.astype(F32)).astype(BF16)
        mean = jnp.dot(high, spread, preferred_element_type=F32) + jnp.dot(
            low, spread, preferred_element_type=F32
        )
        outs.append((part * lax.rsqrt(mean + norm_eps) * gain).astype(BF16))
    return outs[0] if len(outs) == 1 else jnp.concatenate(outs, axis=1)


def body(
    n_sp, n_tp,
    stream, attn_gain_in, w_query, w_key, w_value, w_out, query_gain_in, key_gain_in, rel_bias_in,
    out,
    attn_gain, query_gain, key_gain, rel_bias,
    cur0, cur1, normed, wq, wk, wv, wo, queries, pair_made, halo, kdup, vdup, bias, mixed,
    psend, precv, own0, xsend, xrecv,
    psend1, precv1, own1, xsend1, xrecv1,
    w_sem, ps_sem, pr_sem, xs_sem, xr_sem, cs_sem, cr_sem, hs_sem, hr_sem,
    ps1_sem, pr1_sem, xs1_sem, xr1_sem,
):
    row_count, width = cur0.shape
    segs = row_count // SEG
    half = segs // 2
    q_width = wq.shape[2]
    kv_width = wk.shape[2]
    heads = q_width // HEAD_DIM
    kv_heads = kv_width // HEAD_DIM
    group = heads // kv_heads
    n_x = n_tp // 2
    feat = width // n_tp
    me_sp = lax.axis_index("sp")
    me_tp = lax.axis_index("tp")
    core = lax.rem(me_tp, 2)
    chip = lax.div(me_tp, 2)
    partner = {"tp": chip * 2 + 1 - core}

    def chip_at(k):
        return lax.rem(chip + k, n_x)

    def peer(k):
        return {"tp": chip_at(k) * 2 + core}

    barrier = pltpu.get_barrier_semaphore()
    pl.semaphore_signal(barrier, inc=1, device_id=partner, device_id_type=pl.DeviceIdType.MESH)
    for k in range(1, n_x):
        pl.semaphore_signal(barrier, inc=1, device_id=peer(k), device_id_type=pl.DeviceIdType.MESH)

    @pl.when(me_sp > 0)
    def _():
        pl.semaphore_signal(
            barrier, inc=1, device_id={"sp": me_sp - 1}, device_id_type=pl.DeviceIdType.MESH
        )

    @pl.when(me_sp < n_sp - 1)
    def _():
        pl.semaphore_signal(
            barrier, inc=1, device_id={"sp": me_sp + 1}, device_id_type=pl.DeviceIdType.MESH
        )

    loads = []

    def load(src, dst):
        copy = pltpu.make_async_copy(src, dst, w_sem.at[len(loads)])
        copy.start()
        loads.append(copy)
        return copy

    part_rows = row_count // 2
    parts = [pl.ds(n * part_rows, part_rows) for n in (1, 0)]
    stream_loads = [load(stream.at[part], cur0.at[part]) for part in parts]
    gain_loads = [
        load(attn_gain_in, attn_gain),
        load(query_gain_in, query_gain),
        load(key_gain_in, key_gain),
        load(rel_bias_in, rel_bias),
    ]
    weight_loads = []
    for l in range(LAYERS):
        weight_loads.append(
            [
                load(w_key.at[l], wk.at[l]),
                load(w_value.at[l], wv.at[l]),
                load(w_query.at[l], wq.at[l]),
                load(w_out.at[l], wo.at[l]),
            ]
        )

    def build_bias(l):
        offset = lax.broadcasted_iota(jnp.int32, (2 * CLIP, LINE), 1)
        distance = jnp.clip(LEFT * SEG + SEG - 1 - offset, -CLIP, CLIP) + CLIP
        onehot = (lax.broadcasted_iota(jnp.int32, (2 * CLIP, LINE), 0) == distance).astype(F32)
        far = (distance[:1] == 2 * CLIP).astype(F32)
        table = rel_bias[l]
        line = jnp.dot(
            table[:, : 2 * CLIP], onehot, precision=lax.Precision.HIGHEST, preferred_element_type=F32
        ) + table[:, 2 * CLIP :] * far
        for h in range(heads):
            spread = jnp.broadcast_to(line[h : h + 1], (SEG, LINE))
            turned = pltpu.roll(spread, LINE - (SEG - 1), 1, stride=1, stride_axis=0)
            bias[l, h * SEG : (h + 1) * SEG, :] = turned

    for kv in range(kv_heads):
        vdup[kv, :, 128:] = jnp.ones((2 * row_count, 128), BF16)

    def keys_values(l, rows_in):
        both = jnp.concatenate([wk[l], wv[l]], axis=1)
        flat = jnp.dot(rows_in, both, preferred_element_type=F32)
        keys = head_norm(flat[:, :kv_width], key_gain[l : l + 1], 1.0)
        return keys, flat[:, kv_width:].astype(BF16)

    def make_queries(l, rows_in):
        flat = jnp.dot(rows_in, wq[l], preferred_element_type=F32)
        return head_norm(flat, query_gain[l : l + 1], HEAD_DIM ** (-0.5))

    def put_dup(keys, values, rows):
        for kv in range(kv_heads):
            cols = slice(kv * HEAD_DIM, (kv + 1) * HEAD_DIM)
            kdup[kv, rows, :] = jnp.concatenate([keys[:, cols]] * 2, axis=1)
            vdup[kv, rows, :128] = jnp.concatenate([values[:, cols]] * 2, axis=1)

    def halo_copy(l, seg):
        rows = seg_rows(seg)
        return send(
            pair_made.at[l, rows],
            halo.at[l, rows],
            hs_sem.at[l, seg],
            hr_sem.at[l, seg],
            {"sp": lax.rem(me_sp + 1, n_sp)},
        )

    def start_halo(l, which):
        @pl.when(me_sp < n_sp - 1)
        def _():
            for seg in which:
                halo_copy(l, seg).start()

    def finish_halo(l, seg):
        @pl.when(me_sp > 0)
        def _():
            halo_copy(l, seg).wait_recv()
            got = halo[l, seg_rows(seg), :]
            put_dup(got[:, :kv_width], got[:, kv_width:], seg_rows(seg))

        @pl.when(me_sp == 0)
        def _():
            none = jnp.zeros((SEG, kv_width), BF16)
            put_dup(none, none, seg_rows(seg))

    def end_halo_sends(l):
        @pl.when(me_sp < n_sp - 1)
        def _():
            for seg in range(segs):
                halo_copy(l, seg).wait_send()

    lane = lax.broadcasted_iota(jnp.int32, (SEG, 128), 1)
    low_half = lane < HEAD_DIM

    def attend(l, seg):
        rows = seg_rows(seg)
        window = pl.ds(pl.multiple_of(seg * SEG, SEG), SPAN)
        key_pos = lax.broadcasted_iota(jnp.int32, (1, SPAN), 1)
        inside = me_sp * row_count + (seg - LEFT) * SEG + key_pos >= 0
        shut = jnp.where(inside, 0.0, masked_score)
        for kv in range(kv_heads):
            stack = []
            for p in range(group // 2):
                lower = (kv * group + 2 * p) * HEAD_DIM
                tile = queries[rows, lower : lower + 128]
                none = jnp.zeros_like(tile)
                stack += [jnp.where(low_half, tile, none), jnp.where(low_half, none, tile)]
            stacked = jnp.concatenate(stack, axis=0)
            scores = lax.dot_general(
                stacked, kdup[kv, window, :], (((1,), (1,)), ((), ())), preferred_element_type=F32
            )
            base = kv * group * SEG
            scores = scores + bias[l, base : base + group * SEG, :SPAN] + shut
            peak = jnp.max(scores, axis=-1, keepdims=True)
            expon = jnp.exp(scores - peak).astype(BF16)
            summed = jnp.dot(expon, vdup[kv, window, :], preferred_element_type=F32)
            made = summed[:, :128] / summed[:, 128:]
            for p in range(group // 2):
                lower = (kv * group + 2 * p) * HEAD_DIM
                even = made[2 * p * SEG : (2 * p + 1) * SEG]
                odd = made[(2 * p + 1) * SEG : (2 * p + 2) * SEG]
                mixed[:, lower : lower + 128] = jnp.where(low_half, even, odd).astype(BF16)

    def project_out(l, lower, size):
        cols = pl.ds(pl.multiple_of(lower, 128), size)
        return jnp.dot(mixed[...], wo[l, :, cols], preferred_element_type=F32)

    def meet():
        at_edge = jnp.logical_or(me_sp == 0, me_sp == n_sp - 1)

        @pl.when(at_edge)
        def _():
            pl.semaphore_wait(barrier, n_x + min(n_sp - 1, 1))

        @pl.when(jnp.logical_not(at_edge))
        def _():
            pl.semaphore_wait(barrier, n_x + 2)

    for n, part in enumerate(parts):
        stream_loads[n].wait()
        if n == 0:
            gain_loads[0].wait()
        normed[part, :] = row_norm(cur0[part, :].astype(F32), attn_gain[0:1])
        if n == 0:
            for copy in gain_loads[1:]:
                copy.wait()
            weight_loads[0][0].wait()
            weight_loads[0][1].wait()
        keys, values = keys_values(0, normed[part, :])
        pair_made[0, part, :] = jnp.concatenate([keys, values], axis=1)
        if n == 0:
            meet()
        first_seg = (1 - n) * (segs // 2)
        start_halo(0, reversed(range(first_seg, first_seg + segs // 2)))
        put_dup(keys, values, pl.ds(row_count + (1 - n) * part_rows, part_rows))
    weight_loads[0][2].wait()
    queries[...] = make_queries(0, normed[...])
    build_bias(0)
    weight_loads[0][3].wait()

    def mine_at(i):
        return (half - 1 - i) * 2 + core

    def theirs_at(i):
        return (half - 1 - i) * 2 + 1 - core

    def partner_copy(i):
        return send(psend.at[i], precv.at[i], ps_sem.at[i], pr_sem.at[i], partner)

    sub = SEG // SUBS

    def chip_copy(i, j, k):
        rows = pl.ds(j * sub, sub)
        return send(
            xsend.at[i, rows],
            xrecv.at[k - 1, i, rows],
            xs_sem.at[k - 1, i, j],
            xr_sem.at[k - 1, i, j],
            peer(k),
        )

    def sub_rows(seg, j):
        return pl.ds(pl.multiple_of(seg * SEG + j * sub, sub), sub)

    def rows_copy(i, j, seg):
        rows = sub_rows(seg, j)
        return send(cur1.at[rows], cur1.at[rows], cs_sem.at[i, j], cr_sem.at[i, j], partner)

    out_step = min(width, 512)

    def first_out(i, carry):
        finish_halo(0, (half - 1 - i) * 2 + 1)
        finish_halo(0, (half - 1 - i) * 2)
        attend(0, theirs_at(i))
        for lower in range(0, width, out_step):
            psend[i, :, lower : lower + out_step] = project_out(0, lower, out_step).astype(BF16)
        partner_copy(i).start()
        attend(0, mine_at(i))
        for lower in range(0, width, out_step):
            own0[i, :, lower : lower + out_step] = project_out(0, lower, out_step)
        partner_copy(i).wait_recv()
        for j in range(SUBS):
            rows = slice(j * sub, (j + 1) * sub)
            both = own0[i, rows, :] + precv[i, rows, :].astype(F32)
            own0[i, rows, :] = both
            xsend[i, rows, :] = both.astype(BF16)
            for k in range(1, n_x):
                chip_copy(i, j, k).start()
        return carry

    lax.fori_loop(0, half, first_out, 0)
    build_bias(1)

    for l in range(1, LAYERS):
        for copy in weight_loads[l]:
            copy.wait()

    for i in range(half):
        mine = mine_at(i)
        theirs = theirs_at(i)
        for j in range(SUBS):
            total = own0[i, j * sub : (j + 1) * sub, :]
            for k in range(1, n_x):
                chip_copy(i, j, k).wait_recv()
                total = total + xrecv[k - 1, i, j * sub : (j + 1) * sub, :].astype(F32)
            rows = sub_rows(mine, j)
            summed = (cur0[rows, :].astype(F32) + total).astype(BF16)
            cur1[rows, :] = summed
            rows_copy(i, j, mine).start()
            normed[j * sub : (j + 1) * sub, :] = row_norm(summed.astype(F32), attn_gain[1:2])
        for j in range(SUBS):
            rows_copy(i, j, theirs).wait_recv()
            normed[SEG + j * sub : SEG + (j + 1) * sub, :] = row_norm(
                cur1[sub_rows(theirs, j), :].astype(F32), attn_gain[1:2]
            )
        rows_in = normed[0 : 2 * SEG, :]
        keys, values = keys_values(1, rows_in)
        made = jnp.concatenate([keys, values], axis=1)
        for n, seg in enumerate((mine, theirs)):
            part = slice(n * SEG, (n + 1) * SEG)
            pair_made[1, seg_rows(seg), :] = made[part]
        start_halo(1, (mine, theirs))
        for n, seg in enumerate((mine, theirs)):
            part = slice(n * SEG, (n + 1) * SEG)
            put_dup(keys[part], values[part], seg_rows(seg + segs))
        made_q = make_queries(1, rows_in)
        for n, seg in enumerate((mine, theirs)):
            queries[seg_rows(seg), :] = made_q[n * SEG : (n + 1) * SEG]

    def partner_copy1(s):
        return send(psend1.at[s], precv1.at[s], ps1_sem.at[s], pr1_sem.at[s], partner)

    def chip_copy1(s, k):
        return send(
            xsend1.at[k - 1, s],
            xrecv1.at[k - 1, s],
            xs1_sem.at[k - 1, s],
            xr1_sem.at[k - 1, s],
            peer(k),
        )

    def last_sends(s):
        partner_copy1(s).wait_recv()
        for k in range(n_x):
            both = own1[s, k] + precv1[s, k].astype(F32)
            if k == 0:
                own1[s, k] = both
            else:
                xsend1[k - 1, s] = both.astype(BF16)
                chip_copy1(s, k).start()

    def last_out(s, carry):
        finish_halo(1, segs - 1 - s)
        attend(1, segs - 1 - s)
        for k in range(n_x):
            lower = (chip_at(k) * 2 + 1 - core) * feat
            psend1[s, k] = project_out(1, lower, feat).astype(BF16)
        partner_copy1(s).start()
        for k in range(n_x):
            lower = (chip_at(k) * 2 + core) * feat
            own1[s, k] = project_out(1, lower, feat)

        @pl.when(s > 0)
        def _():
            last_sends(s - 1)

        return carry

    lax.fori_loop(0, segs, last_out, 0)
    last_sends(segs - 1)
    my_cols = pl.ds(pl.multiple_of(me_tp * feat, 128), feat)
    for s in range(segs):
        rows = slice((segs - 1 - s) * SEG, (segs - s) * SEG)
        total = own1[s, 0]
        for k in range(1, n_x):
            chip_copy1(s, k).wait_recv()
            total = total + xrecv1[k - 1, s].astype(F32)
        out[rows, :] = (cur1[rows, my_cols].astype(F32) + total).astype(BF16)

    for i in range(half):
        partner_copy(i).wait_send()
        for j in range(SUBS):
            rows_copy(i, j, mine_at(i)).wait_send()
            for k in range(1, n_x):
                chip_copy(i, j, k).wait_send()
    for s in range(segs):
        partner_copy1(s).wait_send()
        for k in range(1, n_x):
            chip_copy1(s, k).wait_send()
    for l in range(LAYERS):
        end_halo_sends(l)


def local(n_sp, n_tp, stream, attn_gain, w_query, w_key, w_value, w_out, query_gain, key_gain, rel_bias):
    row_count, width = stream.shape
    segs = row_count // SEG
    assert row_count == LEFT * SEG and n_tp % 2 == 0
    half = segs // 2
    n_x = n_tp // 2
    feat = width // n_tp
    q_width = w_query.shape[2]
    kv_width = w_key.shape[2]
    kv_heads = kv_width // HEAD_DIM
    heads = q_width // HEAD_DIM
    others = max(n_x - 1, 1)
    dma = pltpu.SemaphoreType.DMA
    anyw = pl.BlockSpec(memory_space=pltpu.HBM)
    vmem = pl.BlockSpec(memory_space=pltpu.VMEM)
    scratch = [
        pltpu.VMEM(attn_gain.shape, F32),
        pltpu.VMEM(query_gain.shape, F32),
        pltpu.VMEM(key_gain.shape, F32),
        pltpu.VMEM(rel_bias.shape, F32),
        pltpu.VMEM((row_count, width), BF16),
        pltpu.VMEM((row_count, width), BF16),
        pltpu.VMEM((row_count, width), BF16),
        pltpu.VMEM(w_query.shape, BF16),
        pltpu.VMEM(w_key.shape, BF16),
        pltpu.VMEM(w_value.shape, BF16),
        pltpu.VMEM(w_out.shape, BF16),
        pltpu.VMEM((row_count, q_width), BF16),
        pltpu.VMEM((LAYERS, row_count, 2 * kv_width), BF16),
        pltpu.VMEM((LAYERS, row_count, 2 * kv_width), BF16),
        pltpu.VMEM((kv_heads, 2 * row_count, 128), BF16),
        pltpu.VMEM((kv_heads, 2 * row_count, 256), BF16),
        pltpu.VMEM((LAYERS, heads * SEG, LINE), F32),
        pltpu.VMEM((SEG, q_width), BF16),
        pltpu.VMEM((half, SEG, width), BF16),
        pltpu.VMEM((half, SEG, width), BF16),
        pltpu.VMEM((half, SEG, width), F32),
        pltpu.VMEM((half, SEG, width), BF16),
        pltpu.VMEM((others, half, SEG, width), BF16),
        pltpu.VMEM((segs, n_x, SEG, feat), BF16),
        pltpu.VMEM((segs, n_x, SEG, feat), BF16),
        pltpu.VMEM((segs, n_x, SEG, feat), F32),
        pltpu.VMEM((others, segs, SEG, feat), BF16),
        pltpu.VMEM((others, segs, SEG, feat), BF16),
        dma((6 + 4 * LAYERS,)),
        dma((half,)), dma((half,)),
        dma((others, half, SUBS)), dma((others, half, SUBS)),
        dma((half, SUBS)), dma((half, SUBS)),
        dma((LAYERS, segs)), dma((LAYERS, segs)),
        dma((segs,)), dma((segs,)),
        dma((others, segs)), dma((others, segs)),
    ]
    return pl.pallas_call(
        functools.partial(body, n_sp, n_tp),
        out_shape=pltpu.VMEM((row_count, feat), BF16),
        in_specs=[anyw] * 9,
        out_specs=vmem,
        scratch_shapes=scratch,
        compiler_params=pltpu.CompilerParams(
            collective_id=0, has_side_effects=True, vmem_limit_bytes=60 * 1024 * 1024
        ),
    )(stream, attn_gain, w_query, w_key, w_value, w_out, query_gain, key_gain, rel_bias)


def solution(mesh):
    return jax.shard_map(
        functools.partial(local, mesh.shape["sp"], mesh.shape["tp"]),
        mesh=mesh,
        in_specs=(
            P("sp", None),
            P(),
            P(None, None, "tp"),
            P(None, None, "tp"),
            P(None, None, "tp"),
            P(None, "tp", None),
            P(),
            P(),
            P(None, "tp", None),
        ),
        out_specs=P("sp", "tp"),
        check_vma=False,
    )
```

profile of v0, /device:TPU:19, one launch (start us, length us, event | category | flops | bytes accessed | tf_op | source)
XLA Modules:
  0.0 36.8 jit_solution(1946438398628161356)
XLA Ops:
  0.0 36.1 %shard_map.91 = bf16[256,512]{1,0:T(8,128)(2,1)S(1)} custom-call(bf16[256,2048]{1,0:T(8,128)(2,1)} %stream.1, f32[2,2048]{1,0:T(2,128)} %attn_gain_in.1, bf16[2,2048,512]{2,1,0:T(8,128)(2,1)} %w_query.1, bf16[2,2048,128]{2,1,0:T(8,128)(2,1)} %w_key.1, bf16[2,2048,128]{2,1,0:T(8,128)(2,1)} %w_value.1, bf16[2,512,2048]{2,1,0:T(8,128)(2,1)} %w_out.1, ...), custom_call_target="tpu_custom_call" | custom-call | tf_op jit(solution)/shard_map/pallas_call | solution.py:484
  36.1 0.7 %copy.11 = bf16[256,512]{1,0:T(8,128)(2,1)} copy(bf16[256,512]{1,0:T(8,128)(2,1)S(1)} %shard_map.91) | data formatting | bytes 524288
where the time goes:
time: 37 us; the launch traced here: 36.8 us
  Pallas kernels  36.1 us (98%)
  local copies, waits for them, and re-layouts  0.71 us (2%)
    pallas_call x1, Pallas kernels, local(): pl.pallas_call(functools.partial(body, n_sp, n_tp), out_shape=pltpu.VMEM(...  36.1 us

commit v1 on v0

v1 whole, which is shorter than its diff:
```python
import functools

import jax
import jax.numpy as jnp
from jax import lax
from jax.experimental import pallas as pl
from jax.experimental.pallas import tpu as pltpu
from jax.sharding import PartitionSpec as P

HEAD_DIM = 64
SEG = 64
LEFT = 4
CLIP = 128
LAYERS = 2
SPAN = (LEFT + 1) * SEG
LINE = 384
LOG2E = 1.4426950408889634

norm_eps = 1e-06
masked_score = -1e30
F32 = jnp.float32
BF16 = jnp.bfloat16


def seg_rows(seg):
    return pl.ds(pl.multiple_of(seg * SEG, SEG), SEG)


def send(src, dst, send_sem, recv_sem, device):
    return pltpu.make_async_remote_copy(
        src_ref=src,
        dst_ref=dst,
        send_sem=send_sem,
        recv_sem=recv_sem,
        device_id=device,
        device_id_type=pl.DeviceIdType.MESH,
    )


def row_norm(x, gain):
    squared = jnp.mean(x * x, axis=-1, keepdims=True)
    return (x * lax.rsqrt(squared + norm_eps) * gain).astype(BF16)


def head_norm(x, gain_row, scale):
    width = x.shape[1]
    block = min(width, 256)
    row_head = lax.broadcasted_iota(jnp.int32, (block, block), 0) >> 6
    col_head = lax.broadcasted_iota(jnp.int32, (block, block), 1) >> 6
    spread = jnp.where(row_head == col_head, 1.0 / HEAD_DIM, 0.0).astype(BF16)
    gain = jnp.concatenate([gain_row] * (block // HEAD_DIM), axis=1) * scale
    outs = []
    for lower in range(0, width, block):
        part = x[:, lower : lower + block]
        squares = part * part
        high = squares.astype(BF16)
        low = (squares - high.astype(F32)).astype(BF16)
        mean = jnp.dot(high, spread, preferred_element_type=F32) + jnp.dot(
            low, spread, preferred_element_type=F32
        )
        outs.append((part * lax.rsqrt(mean + norm_eps) * gain).astype(BF16))
    return outs[0] if len(outs) == 1 else jnp.concatenate(outs, axis=1)


def body(
    n_sp, n_tp,
    stream, attn_gain_in, w_query, w_key, w_value, w_out, query_gain_in, key_gain_in, rel_bias_in,
    out,
    attn_gain, query_gain, key_gain, rel_bias,
    cur0, cur1, normed, wq, wk, wv, wo, queries, pair_made, halo, kdup, vdup, bias, ahead, mixed,
    psend, precv, own0, xsend, xrecv,
    psend1, precv1, own1, xsend1, xrecv1,
    w_sem, ps_sem, pr_sem, xs_sem, xr_sem, cs_sem, cr_sem, hs_sem, hr_sem,
    ps1_sem, xs1_sem, xr1_sem,
):
    row_count, width = cur0.shape
    segs = row_count // SEG
    q_width = wq.shape[2]
    kv_width = wk.shape[2]
    heads = q_width // HEAD_DIM
    kv_heads = kv_width // HEAD_DIM
    group = heads // kv_heads
    n_x = n_tp // 2
    feat = width // n_tp
    half_width = width // 2
    last = segs - 1
    me_sp = lax.axis_index("sp")
    me_tp = lax.axis_index("tp")
    core = lax.rem(me_tp, 2)
    chip = lax.div(me_tp, 2)
    partner = {"tp": chip * 2 + 1 - core}

    def chip_at(k):
        return lax.rem(chip + k, n_x)

    def peer(k):
        return {"tp": chip_at(k) * 2 + core}

    barrier = pltpu.get_barrier_semaphore()
    pl.semaphore_signal(barrier, inc=1, device_id=partner, device_id_type=pl.DeviceIdType.MESH)
    for k in range(1, n_x):
        pl.semaphore_signal(barrier, inc=1, device_id=peer(k), device_id_type=pl.DeviceIdType.MESH)

    @pl.when(me_sp > 0)
    def _():
        pl.semaphore_signal(
            barrier, inc=1, device_id={"sp": me_sp - 1}, device_id_type=pl.DeviceIdType.MESH
        )

    @pl.when(me_sp < n_sp - 1)
    def _():
        pl.semaphore_signal(
            barrier, inc=1, device_id={"sp": me_sp + 1}, device_id_type=pl.DeviceIdType.MESH
        )

    def load(n, src, dst):
        copy = pltpu.make_async_copy(src, dst, w_sem.at[n])
        copy.start()
        return copy

    early = pl.ds(last * SEG, SEG)
    late = pl.ds(0, last * SEG)
    early_load = load(0, stream.at[early], cur0.at[early])
    attn_gain_load = load(1, attn_gain_in, attn_gain)
    wk_load = load(2, w_key.at[0], wk.at[0])
    wv_load = load(3, w_value.at[0], wv.at[0])
    key_gain_load = load(4, key_gain_in, key_gain)
    late_load = load(5, stream.at[late], cur0.at[late])
    rel_bias_load = load(6, rel_bias_in, rel_bias)
    query_gain_load = load(7, query_gain_in, query_gain)
    wq_load = load(8, w_query.at[0], wq.at[0])
    wo_load = load(9, w_out.at[0], wo.at[0])

    low_half = lax.broadcasted_iota(jnp.int32, (SEG, 128), 1) < HEAD_DIM

    def build_bias(l):
        offset = lax.broadcasted_iota(jnp.int32, (2 * CLIP, LINE), 1)
        distance = jnp.clip(LEFT * SEG + SEG - 1 - offset, -CLIP, CLIP) + CLIP
        onehot = (lax.broadcasted_iota(jnp.int32, (2 * CLIP, LINE), 0) == distance).astype(F32)
        far = (distance[:1] == 2 * CLIP).astype(F32)
        table = rel_bias[l]
        line = jnp.dot(
            table[:, : 2 * CLIP], onehot, precision=lax.Precision.HIGHEST, preferred_element_type=F32
        ) + table[:, 2 * CLIP :] * far
        shut = jnp.where(me_sp == 0, masked_score, 0.0)
        shut_low = jnp.where(low_half, shut, 0.0)
        shut_high = jnp.where(low_half, 0.0, shut)
        for h in range(heads):
            spread = jnp.broadcast_to(line[h : h + 1], (SEG, LINE))
            turned = pltpu.roll(spread, LINE - (SEG - 1), 1, stride=1, stride_axis=0)
            moved = pltpu.roll(turned, LINE - SEG, 1)
            plain = [turned[:, n * 128 : (n + 1) * 128] for n in range(3)]
            other = [moved[:, n * 128 : (n + 1) * 128] for n in range(3)]

            def in_low(w):
                return other[w // 2] if w % 2 else plain[w // 2]

            def in_high(w):
                return plain[w // 2] if w % 2 else other[(w // 2 - 1) % 3]

            for seg in range(segs):
                own = LEFT - seg
                if l == 0 and seg == last:
                    order = list(range(own + 1, LEFT + 1)) + [own] + list(range(own))
                else:
                    order = [w for w in range(LEFT + 1) if w != own] + [own]
                tiles = []
                for n in range(3):
                    w = order[2 * n]
                    tile = in_low(w)
                    if n < 2:
                        v = order[2 * n + 1]
                        if in_high(v) is not tile:
                            tile = jnp.where(low_half, tile, in_high(v))
                        if w < own and v < own:
                            tile = tile + shut
                        elif w < own:
                            tile = tile + shut_low
                        elif v < own:
                            tile = tile + shut_high
                    else:
                        if w < own:
                            tile = tile + shut
                        tile = jnp.where(low_half, tile, masked_score)
                    tiles.append(tile)
                top = jnp.maximum(jnp.maximum(tiles[0], tiles[1]), tiles[2])
                peak = jnp.max(top, axis=-1, keepdims=True)
                for n in range(3):
                    bias[l, seg, h * SEG : (h + 1) * SEG, n * 128 : (n + 1) * 128] = (
                        tiles[n] - peak
                    ) * LOG2E

    for kv in range(kv_heads):
        vdup[kv, :, 128:] = jnp.ones((2 * row_count, 128), BF16)

    def keys_values(l, rows_in):
        both = jnp.concatenate([wk[l], wv[l]], axis=1)
        flat = jnp.dot(rows_in, both, preferred_element_type=F32)
        keys = head_norm(flat[:, :kv_width], key_gain[l : l + 1], 1.0)
        return keys, flat[:, kv_width:].astype(BF16)

    def make_queries(l, rows_in):
        flat = jnp.dot(rows_in, wq[l], preferred_element_type=F32)
        return head_norm(flat, query_gain[l : l + 1], HEAD_DIM ** (-0.5) * LOG2E)

    def place(seg):
        return row_count + lax.rem(seg + last, segs) * SEG

    def put_dup(keys, values, rows):
        for kv in range(kv_heads):
            cols = slice(kv * HEAD_DIM, (kv + 1) * HEAD_DIM)
            kdup[kv, rows, :] = jnp.concatenate([keys[:, cols]] * 2, axis=1)
            vdup[kv, rows, :128] = jnp.concatenate([values[:, cols]] * 2, axis=1)

    def halo_copy(l, seg):
        rows = seg_rows(seg)
        return send(
            pair_made.at[l, rows],
            halo.at[l, rows],
            hs_sem.at[l],
            hr_sem.at[l, seg],
            {"sp": lax.rem(me_sp + 1, n_sp)},
        )

    def start_halo(l, which):
        @pl.when(me_sp < n_sp - 1)
        def _():
            for seg in which:
                halo_copy(l, seg).start()

    def finish_halo(l, seg):
        @pl.when(me_sp > 0)
        def _():
            halo_copy(l, seg).wait_recv()
            got = halo[l, seg_rows(seg), :]
            put_dup(got[:, :kv_width], got[:, kv_width:], seg_rows(seg))

        @pl.when(me_sp == 0)
        def _():
            none = jnp.zeros((SEG, kv_width), BF16)
            put_dup(none, none, seg_rows(seg))

    main = LEFT * SEG
    tail_rows = pl.ds(2 * row_count - SEG, SEG)

    def attend_part(l, seg, kv, rows_at, lanes):
        rows = seg_rows(seg)
        stack = []
        for p in range(group // 2):
            lower = (kv * group + 2 * p) * HEAD_DIM
            tile = queries[rows, lower : lower + 128]
            none = jnp.zeros_like(tile)
            stack += [jnp.where(low_half, tile, none), jnp.where(low_half, none, tile)]
        stacked = jnp.concatenate(stack, axis=0)
        scores = lax.dot_general(
            stacked, kdup[kv, rows_at, :], (((1,), (1,)), ((), ())), preferred_element_type=F32
        )
        base = kv * group * SEG
        expon = jnp.exp2(scores + bias[l, seg, base : base + group * SEG, lanes]).astype(BF16)
        return jnp.dot(expon, vdup[kv, rows_at, :], preferred_element_type=F32)

    def put_mixed(kv, summed):
        for p in range(group // 2):
            lower = (kv * group + 2 * p) * HEAD_DIM
            even = summed[2 * p * SEG : (2 * p + 1) * SEG]
            odd = summed[(2 * p + 1) * SEG : (2 * p + 2) * SEG]
            top = jnp.where(low_half, even[:, :128], odd[:, :128])
            under = jnp.where(low_half, even[:, 128:], odd[:, 128:])
            mixed[:, lower : lower + 128] = (top / under).astype(BF16)

    def attend(l, seg):
        window = pl.ds(pl.multiple_of(seg * SEG, SEG), main)
        for kv in range(kv_heads):
            put_mixed(
                kv,
                attend_part(l, seg, kv, window, slice(0, main))
                + attend_part(l, seg, kv, tail_rows, slice(main, SPAN)),
            )

    def attend_ahead(l, rows_at):
        for kv in range(kv_heads):
            ahead[kv] = attend_part(l, last, kv, rows_at, slice(0, main))

    def attend_rest(l, rows_at):
        for kv in range(kv_heads):
            put_mixed(kv, ahead[kv] + attend_part(l, last, kv, rows_at, slice(main, SPAN)))

    def project_out(l, lower, size):
        cols = pl.ds(pl.multiple_of(lower, 128), size)
        return jnp.dot(mixed[...], wo[l, :, cols], preferred_element_type=F32)

    def meet():
        at_edge = jnp.logical_or(me_sp == 0, me_sp == n_sp - 1)

        @pl.when(at_edge)
        def _():
            pl.semaphore_wait(barrier, n_x + min(n_sp - 1, 1))

        @pl.when(jnp.logical_not(at_edge))
        def _():
            pl.semaphore_wait(barrier, n_x + 2)

    early_load.wait()
    attn_gain_load.wait()
    normed[early, :] = row_norm(cur0[early, :].astype(F32), attn_gain[0:1])
    wk_load.wait()
    wv_load.wait()
    key_gain_load.wait()
    keys, values = keys_values(0, normed[early, :])
    pair_made[0, early, :] = jnp.concatenate([keys, values], axis=1)
    meet()
    start_halo(0, [last])
    put_dup(keys, values, pl.ds(2 * row_count - 2 * SEG, SEG))
    late_load.wait()
    normed[late, :] = row_norm(cur0[late, :].astype(F32), attn_gain[0:1])
    keys, values = keys_values(0, normed[late, :])
    pair_made[0, late, :] = jnp.concatenate([keys, values], axis=1)
    start_halo(0, reversed(range(last)))
    put_dup(keys[:SEG], values[:SEG], tail_rows)
    put_dup(keys[SEG:], values[SEG:], pl.ds(row_count, (last - 1) * SEG))
    rel_bias_load.wait()
    query_gain_load.wait()
    wq_load.wait()
    queries[...] = make_queries(0, normed[...])
    build_bias(0)
    wo_load.wait()
    second_loads = [
        load(2, w_key.at[1], wk.at[1]),
        load(3, w_value.at[1], wv.at[1]),
        load(8, w_query.at[1], wq.at[1]),
        load(9, w_out.at[1], wo.at[1]),
    ]

    def partner_copy(i):
        return send(psend.at[i], precv.at[i], ps_sem.at[0], pr_sem.at[i], partner)

    def chip_copy(i, k):
        return send(
            xsend.at[i], xrecv.at[k - 1, i], xs_sem.at[k - 1], xr_sem.at[k - 1, i], peer(k)
        )

    my_half = pl.ds(pl.multiple_of(core * half_width, 128), half_width)

    def rows_copy(i, seg):
        rows = seg_rows(seg)
        return send(
            cur1.at[rows, my_half], cur1.at[rows, my_half], cs_sem.at[0], cr_sem.at[i], partner
        )

    out_step = min(half_width, 512)

    def first_out(i):
        for lower in range(0, half_width, out_step):
            psend[i, :, lower : lower + out_step] = project_out(
                0, (1 - core) * half_width + lower, out_step
            ).astype(BF16)
        partner_copy(i).start()
        for lower in range(0, half_width, out_step):
            own0[i, :, lower : lower + out_step] = project_out(
                0, core * half_width + lower, out_step
            )
        partner_copy(i).wait_recv()
        both = own0[i] + precv[i].astype(F32)
        own0[i] = both
        xsend[i] = both.astype(BF16)
        for k in range(1, n_x):
            chip_copy(i, k).start()

    attend_ahead(0, pl.ds(row_count, main))
    finish_halo(0, last)
    attend_rest(0, pl.ds(row_count - SEG, SEG))
    first_out(0)

    def first_round(i, carry):
        finish_halo(0, last - i)
        attend(0, last - i)
        first_out(i)
        return carry

    lax.fori_loop(1, segs, first_round, 0)
    build_bias(1)
    for copy in second_loads:
        copy.wait()

    def gather_rows(i, seg):
        rows = seg_rows(seg)
        total = own0[i]
        for k in range(1, n_x):
            chip_copy(i, k).wait_recv()
            total = total + xrecv[k - 1, i].astype(F32)
        cur1[rows, my_half] = (cur0[rows, my_half].astype(F32) + total).astype(BF16)
        rows_copy(i, seg).start()
        rows_copy(i, seg).wait_recv()
        normed[0:SEG, :] = row_norm(cur1[rows, :].astype(F32), attn_gain[1:2])
        return keys_values(1, normed[0:SEG, :])

    def second_queries(seg):
        queries[seg_rows(seg), :] = make_queries(1, normed[0:SEG, :])

    def put_own(keys, values, seg):
        pair_made[1, seg_rows(seg), :] = jnp.concatenate([keys, values], axis=1)
        start_halo(1, [seg])
        put_dup(keys, values, pl.ds(pl.multiple_of(place(seg), SEG), SEG))

    def second_round(i, carry):
        keys, values = gather_rows(i, last - i)
        second_queries(last - i)
        put_own(keys, values, last - i)
        return carry

    lax.fori_loop(0, last, second_round, 0)
    finish_halo(1, last)
    attend_ahead(1, pl.ds(row_count - SEG, main))
    keys, values = gather_rows(last, 0)
    put_own(keys, values, 0)

    def partner_copy1(s):
        return send(psend1.at[s], precv1.at[s], ps1_sem.at[0], pr_sem.at[s], partner)

    def chip_copy1(s, k):
        return send(
            xsend1.at[k - 1, s],
            xrecv1.at[k - 1, s],
            xs1_sem.at[k - 1],
            xr1_sem.at[k - 1, s],
            peer(k),
        )

    def last_partner(s):
        for k in range(n_x):
            lower = (chip_at(k) * 2 + 1 - core) * feat
            psend1[s, k] = project_out(1, lower, feat).astype(BF16)
        partner_copy1(s).start()

    def last_own(s):
        for k in range(n_x):
            lower = (chip_at(k) * 2 + core) * feat
            own1[s, k] = project_out(1, lower, feat)

    def last_sends(s):
        partner_copy1(s).wait_recv()
        for k in range(n_x):
            both = own1[s, k] + precv1[s, k].astype(F32)
            if k == 0:
                own1[s, k] = both
            else:
                xsend1[k - 1, s] = both.astype(BF16)
                chip_copy1(s, k).start()

    attend_rest(1, tail_rows)
    last_partner(0)
    second_queries(0)
    last_own(0)
    last_sends(0)

    def last_round(s, carry):
        finish_halo(1, last - s)
        attend(1, last - s)

        @pl.when(s > 1)
        def _():
            last_sends(s - 1)

        last_partner(s)
        last_own(s)
        return carry

    lax.fori_loop(1, segs, last_round, 0)
    last_sends(last)
    my_cols = pl.ds(pl.multiple_of(me_tp * feat, 128), feat)
    for s in range(segs):
        rows = slice((last - s) * SEG, (segs - s) * SEG)
        total = own1[s, 0]
        for k in range(1, n_x):
            chip_copy1(s, k).wait_recv()
            total = total + xrecv1[k - 1, s].astype(F32)
        out[rows, :] = (cur1[rows, my_cols].astype(F32) + total).astype(BF16)

    send(psend, precv, ps_sem.at[0], pr_sem.at[0], partner).wait_send()
    send(cur1.at[:, my_half], cur1.at[:, my_half], cs_sem.at[0], cr_sem.at[0], partner).wait_send()
    send(psend1, precv1, ps1_sem.at[0], pr_sem.at[0], partner).wait_send()
    for k in range(1, n_x):
        send(xsend, xrecv.at[k - 1], xs_sem.at[k - 1], xr_sem.at[k - 1, 0], peer(k)).wait_send()
        send(
            xsend1.at[k - 1], xrecv1.at[k - 1], xs1_sem.at[k - 1], xr1_sem.at[k - 1, 0], peer(k)
        ).wait_send()

    @pl.when(me_sp < n_sp - 1)
    def _():
        for l in range(LAYERS):
            send(
                pair_made.at[l], halo.at[l], hs_sem.at[l], hr_sem.at[l, 0],
                {"sp": lax.rem(me_sp + 1, n_sp)},
            ).wait_send()


def local(n_sp, n_tp, stream, attn_gain, w_query, w_key, w_value, w_out, query_gain, key_gain, rel_bias):
    row_count, width = stream.shape
    segs = row_count // SEG
    assert row_count == LEFT * SEG and n_tp % 2 == 0
    n_x = n_tp // 2
    feat = width // n_tp
    half_width = width // 2
    q_width = w_query.shape[2]
    kv_width = w_key.shape[2]
    kv_heads = kv_width // HEAD_DIM
    heads = q_width // HEAD_DIM
    group = heads // kv_heads
    others = max(n_x - 1, 1)
    dma = pltpu.SemaphoreType.DMA
    anyw = pl.BlockSpec(memory_space=pltpu.HBM)
    vmem = pl.BlockSpec(memory_space=pltpu.VMEM)
    scratch = [
        pltpu.VMEM(attn_gain.shape, F32),
        pltpu.VMEM(query_gain.shape, F32),
        pltpu.VMEM(key_gain.shape, F32),
        pltpu.VMEM(rel_bias.shape, F32),
        pltpu.VMEM((row_count, width), BF16),
        pltpu.VMEM((row_count, width), BF16),
        pltpu.VMEM((row_count, width), BF16),
        pltpu.VMEM(w_query.shape, BF16),
        pltpu.VMEM(w_key.shape, BF16),
        pltpu.VMEM(w_value.shape, BF16),
        pltpu.VMEM(w_out.shape, BF16),
        pltpu.VMEM((row_count, q_width), BF16),
        pltpu.VMEM((LAYERS, row_count, 2 * kv_width), BF16),
        pltpu.VMEM((LAYERS, row_count, 2 * kv_width), BF16),
        pltpu.VMEM((kv_heads, 2 * row_count, 128), BF16),
        pltpu.VMEM((kv_heads, 2 * row_count, 256), BF16),
        pltpu.VMEM((LAYERS, segs, heads * SEG, LINE), F32),
        pltpu.VMEM((kv_heads, group * SEG, 256), F32),
        pltpu.VMEM((SEG, q_width), BF16),
        pltpu.VMEM((segs, SEG, half_width), BF16),
        pltpu.VMEM((segs, SEG, half_width), BF16),
        pltpu.VMEM((segs, SEG, half_width), F32),
        pltpu.VMEM((segs, SEG, half_width), BF16),
        pltpu.VMEM((others, segs, SEG, half_width), BF16),
        pltpu.VMEM((segs, n_x, SEG, feat), BF16),
        pltpu.VMEM((segs, n_x, SEG, feat), BF16),
        pltpu.VMEM((segs, n_x, SEG, feat), F32),
        pltpu.VMEM((others, segs, SEG, feat), BF16),
        pltpu.VMEM((others, segs, SEG, feat), BF16),
        dma((10,)),
        dma((1,)), dma((segs,)),
        dma((others,)), dma((others, segs)),
        dma((1,)), dma((segs,)),
        dma((LAYERS,)), dma((LAYERS, segs)),
        dma((1,)),
        dma((others,)), dma((others, segs)),
    ]
    return pl.pallas_call(
        functools.partial(body, n_sp, n_tp),
        out_shape=pltpu.VMEM((row_count, feat), BF16),
        in_specs=[anyw] * 9,
        out_specs=vmem,
        scratch_shapes=scratch,
        compiler_params=pltpu.CompilerParams(
            collective_id=0, has_side_effects=True, vmem_limit_bytes=60 * 1024 * 1024
        ),
    )(stream, attn_gain, w_query, w_key, w_value, w_out, query_gain, key_gain, rel_bias)


def solution(mesh):
    return jax.shard_map(
        functools.partial(local, mesh.shape["sp"], mesh.shape["tp"]),
        mesh=mesh,
        in_specs=(
            P("sp", None),
            P(),
            P(None, None, "tp"),
            P(None, None, "tp"),
            P(None, None, "tp"),
            P(None, "tp", None),
            P(),
            P(),
            P(None, "tp", None),
        ),
        out_specs=P("sp", "tp"),
        check_vma=False,
    )
```

time: 37 us -> 37.5 us (1.014)
  the two profiles are of different devices: /device:TPU:19 before, /device:TPU:0 now
where the time goes in v1:
time: 37.5 us; the launch traced here: 37.4 us
  Pallas kernels  36.7 us (98%)
  local copies, waits for them, and re-layouts  0.71 us (2%)
    pallas_call x1, Pallas kernels, local(): pl.pallas_call(functools.partial(body, n_sp, n_tp), out_shape=pltpu.VMEM(...  36.7 us

profile of v1, /device:TPU:0, one launch (start us, length us, event | category | flops | bytes accessed | tf_op | source)
XLA Modules:
  0.0 37.4 jit_solution(6636965665473416760)
XLA Ops:
  0.0 36.7 %shard_map.91 = bf16[256,512]{1,0:T(8,128)(2,1)S(1)} custom-call(bf16[256,2048]{1,0:T(8,128)(2,1)} %stream.1, f32[2,2048]{1,0:T(2,128)} %attn_gain_in.1, bf16[2,2048,512]{2,1,0:T(8,128)(2,1)} %w_query.1, bf16[2,2048,128]{2,1,0:T(8,128)(2,1)} %w_key.1, bf16[2,2048,128]{2,1,0:T(8,128)(2,1)} %w_value.1, bf16[2,512,2048]{2,1,0:T(8,128)(2,1)} %w_out.1, ...), custom_call_target="tpu_custom_call" | custom-call | tf_op jit(solution)/shard_map/pallas_call | solution.py:551
  36.7 0.7 %copy.11 = bf16[256,512]{1,0:T(8,128)(2,1)} copy(bf16[256,512]{1,0:T(8,128)(2,1)S(1)} %shard_map.91) | data formatting | bytes 524288

commit v2 on v1

--- a/solution.py
+++ b/solution.py
@@ -67,7 +67,7 @@
     stream, attn_gain_in, w_query, w_key, w_value, w_out, query_gain_in, key_gain_in, rel_bias_in,
     out,
     attn_gain, query_gain, key_gain, rel_bias,
-    cur0, cur1, normed, wq, wk, wv, wo, queries, pair_made, halo, kdup, vdup, bias, ahead, mixed,
+    cur0, cur1, normed, wq, wk, wv, wo, queries, pair_made, halo, kdup, vdup, line, bias, ahead, mixed,
     psend, precv, own0, xsend, xrecv,
     psend1, precv1, own1, xsend1, xrecv1,
     w_sem, ps_sem, pr_sem, xs_sem, xr_sem, cs_sem, cr_sem, hs_sem, hr_sem,
@@ -120,33 +120,42 @@
 
     early = pl.ds(last * SEG, SEG)
     late = pl.ds(0, last * SEG)
+    rel_bias_load = load(6, rel_bias_in, rel_bias)
     early_load = load(0, stream.at[early], cur0.at[early])
     attn_gain_load = load(1, attn_gain_in, attn_gain)
     wk_load = load(2, w_key.at[0], wk.at[0])
     wv_load = load(3, w_value.at[0], wv.at[0])
     key_gain_load = load(4, key_gain_in, key_gain)
     late_load = load(5, stream.at[late], cur0.at[late])
-    rel_bias_load = load(6, rel_bias_in, rel_bias)
     query_gain_load = load(7, query_gain_in, query_gain)
     wq_load = load(8, w_query.at[0], wq.at[0])
     wo_load = load(9, w_out.at[0], wo.at[0])
 
     low_half = lax.broadcasted_iota(jnp.int32, (SEG, 128), 1) < HEAD_DIM
 
-    def build_bias(l):
+    def build_line():
         offset = lax.broadcasted_iota(jnp.int32, (2 * CLIP, LINE), 1)
         distance = jnp.clip(LEFT * SEG + SEG - 1 - offset, -CLIP, CLIP) + CLIP
-        onehot = (lax.broadcasted_iota(jnp.int32, (2 * CLIP, LINE), 0) == distance).astype(F32)
+        match = lax.broadcasted_iota(jnp.int32, (2 * CLIP, LINE), 0) == distance
+        onehot = jnp.where(match, 1.0, 0.0).astype(BF16)
         far = (distance[:1] == 2 * CLIP).astype(F32)
-        table = rel_bias[l]
-        line = jnp.dot(
-            table[:, : 2 * CLIP], onehot, precision=lax.Precision.HIGHEST, preferred_element_type=F32
-        ) + table[:, 2 * CLIP :] * far
+        table = jnp.concatenate([rel_bias[l] for l in range(LAYERS)], axis=0)
+        near = table[:, : 2 * CLIP]
+        high = near.astype(BF16)
+        near = near - high.astype(F32)
+        middle = near.astype(BF16)
+        low = (near - middle.astype(F32)).astype(BF16)
+        high, middle, low = (
+            jnp.dot(part, onehot, preferred_element_type=F32) for part in (high, middle, low)
+        )
+        line[...] = high + middle + low + table[:, 2 * CLIP :] * far
+
+    def build_bias(l):
         shut = jnp.where(me_sp == 0, masked_score, 0.0)
         shut_low = jnp.where(low_half, shut, 0.0)
         shut_high = jnp.where(low_half, 0.0, shut)
         for h in range(heads):
-            spread = jnp.broadcast_to(line[h : h + 1], (SEG, LINE))
+            spread = jnp.broadcast_to(line[l * heads + h : l * heads + h + 1, :], (SEG, LINE))
             turned = pltpu.roll(spread, LINE - (SEG - 1), 1, stride=1, stride_axis=0)
             moved = pltpu.roll(turned, LINE - SEG, 1)
             plain = [turned[:, n * 128 : (n + 1) * 128] for n in range(3)]
@@ -259,35 +268,38 @@
         expon = jnp.exp2(scores + bias[l, seg, base : base + group * SEG, lanes]).astype(BF16)
         return jnp.dot(expon, vdup[kv, rows_at, :], preferred_element_type=F32)
 
-    def put_mixed(kv, summed):
+    def put_mixed(seg, kv, summed):
+        rows = seg_rows(seg)
         for p in range(group // 2):
             lower = (kv * group + 2 * p) * HEAD_DIM
             even = summed[2 * p * SEG : (2 * p + 1) * SEG]
             odd = summed[(2 * p + 1) * SEG : (2 * p + 2) * SEG]
             top = jnp.where(low_half, even[:, :128], odd[:, :128])
             under = jnp.where(low_half, even[:, 128:], odd[:, 128:])
-            mixed[:, lower : lower + 128] = (top / under).astype(BF16)
+            mixed[rows, lower : lower + 128] = (top / under).astype(BF16)
 
     def attend(l, seg):
         window = pl.ds(pl.multiple_of(seg * SEG, SEG), main)
         for kv in range(kv_heads):
             put_mixed(
+                seg,
                 kv,
                 attend_part(l, seg, kv, window, slice(0, main))
                 + attend_part(l, seg, kv, tail_rows, slice(main, SPAN)),
             )
 
-    def attend_ahead(l, rows_at):
+    def attend_ahead(l, seg, rows_at):
         for kv in range(kv_heads):
-            ahead[kv] = attend_part(l, last, kv, rows_at, slice(0, main))
-
-    def attend_rest(l, rows_at):
+            ahead[last - seg, kv] = attend_part(l, seg, kv, rows_at, slice(0, main))
+
+    def attend_rest(l, seg, rows_at):
         for kv in range(kv_heads):
-            put_mixed(kv, ahead[kv] + attend_part(l, last, kv, rows_at, slice(main, SPAN)))
-
-    def project_out(l, lower, size):
+            rest = attend_part(l, seg, kv, rows_at, slice(main, SPAN))
+            put_mixed(seg, kv, ahead[last - seg, kv] + rest)
+
+    def project_out(l, rows, lower, size):
         cols = pl.ds(pl.multiple_of(lower, 128), size)
-        return jnp.dot(mixed[...], wo[l, :, cols], preferred_element_type=F32)
+        return jnp.dot(mixed[rows, :], wo[l, :, cols], preferred_element_type=F32)
 
     def meet():
         at_edge = jnp.logical_or(me_sp == 0, me_sp == n_sp - 1)
@@ -300,8 +312,10 @@
         def _():
             pl.semaphore_wait(barrier, n_x + 2)
 
+    rel_bias_load.wait()
     early_load.wait()
     attn_gain_load.wait()
+    build_line()
     normed[early, :] = row_norm(cur0[early, :].astype(F32), attn_gain[0:1])
     wk_load.wait()
     wv_load.wait()
@@ -318,12 +332,11 @@
     start_halo(0, reversed(range(last)))
     put_dup(keys[:SEG], values[:SEG], tail_rows)
     put_dup(keys[SEG:], values[SEG:], pl.ds(row_count, (last - 1) * SEG))
-    rel_bias_load.wait()
     query_gain_load.wait()
     wq_load.wait()
+    wo_load.wait()
     queries[...] = make_queries(0, normed[...])
     build_bias(0)
-    wo_load.wait()
     second_loads = [
         load(2, w_key.at[1], wk.at[1]),
         load(3, w_value.at[1], wv.at[1]),
@@ -349,16 +362,20 @@
 
     out_step = min(half_width, 512)
 
-    def first_out(i):
+    def first_partner(i):
         for lower in range(0, half_width, out_step):
             psend[i, :, lower : lower + out_step] = project_out(
-                0, (1 - core) * half_width + lower, out_step
+                0, seg_rows(last - i), (1 - core) * half_width + lower, out_step
             ).astype(BF16)
         partner_copy(i).start()
+
+    def first_own(i):
         for lower in range(0, half_width, out_step):
             own0[i, :, lower : lower + out_step] = project_out(
-                0, core * half_width + lower, out_step
+                0, seg_rows(last - i), core * half_width + lower, out_step
             )
+
+    def first_sends(i):
         partner_copy(i).wait_recv()
         both = own0[i] + precv[i].astype(F32)
         own0[i] = both
@@ -366,21 +383,27 @@
         for k in range(1, n_x):
             chip_copy(i, k).start()
 
-    attend_ahead(0, pl.ds(row_count, main))
+    attend_ahead(0, last, pl.ds(row_count, main))
     finish_halo(0, last)
-    attend_rest(0, pl.ds(row_count - SEG, SEG))
-    first_out(0)
+    attend_rest(0, last, pl.ds(row_count - SEG, SEG))
+    first_partner(0)
+    first_own(0)
+    first_sends(0)
 
     def first_round(i, carry):
         finish_halo(0, last - i)
         attend(0, last - i)
-        first_out(i)
+        first_partner(i)
+
+        @pl.when(i > 1)
+        def _():
+            first_sends(i - 1)
+
+        first_own(i)
         return carry
 
     lax.fori_loop(1, segs, first_round, 0)
-    build_bias(1)
-    for copy in second_loads:
-        copy.wait()
+    first_sends(last)
 
     def gather_rows(i, seg):
         rows = seg_rows(seg)
@@ -390,91 +413,103 @@
             total = total + xrecv[k - 1, i].astype(F32)
         cur1[rows, my_half] = (cur0[rows, my_half].astype(F32) + total).astype(BF16)
         rows_copy(i, seg).start()
+
+    def second_keys(i, seg):
+        rows = seg_rows(seg)
         rows_copy(i, seg).wait_recv()
-        normed[0:SEG, :] = row_norm(cur1[rows, :].astype(F32), attn_gain[1:2])
-        return keys_values(1, normed[0:SEG, :])
-
-    def second_queries(seg):
-        queries[seg_rows(seg), :] = make_queries(1, normed[0:SEG, :])
-
-    def put_own(keys, values, seg):
-        pair_made[1, seg_rows(seg), :] = jnp.concatenate([keys, values], axis=1)
+        normed[rows, :] = row_norm(cur1[rows, :].astype(F32), attn_gain[1:2])
+        keys, values = keys_values(1, normed[rows, :])
+        pair_made[1, rows, :] = jnp.concatenate([keys, values], axis=1)
         start_halo(1, [seg])
         put_dup(keys, values, pl.ds(pl.multiple_of(place(seg), SEG), SEG))
 
+    def second_queries(seg):
+        queries[seg_rows(seg), :] = make_queries(1, normed[seg_rows(seg), :])
+
+    gather_rows(0, last)
+    build_bias(1)
+    for copy in second_loads:
+        copy.wait()
+    second_keys(0, last)
+
     def second_round(i, carry):
-        keys, values = gather_rows(i, last - i)
-        second_queries(last - i)
-        put_own(keys, values, last - i)
+        gather_rows(i, last - i)
+        second_queries(segs - i)
+        second_keys(i, last - i)
         return carry
 
-    lax.fori_loop(0, last, second_round, 0)
-    finish_halo(1, last)
-    attend_ahead(1, pl.ds(row_count - SEG, main))
-    keys, values = gather_rows(last, 0)
-    put_own(keys, values, 0)
-
-    def partner_copy1(s):
-        return send(psend1.at[s], precv1.at[s], ps1_sem.at[0], pr_sem.at[s], partner)
-
-    def chip_copy1(s, k):
+    lax.fori_loop(1, last, second_round, 0)
+    second_queries(1)
+    gather_rows(last, 0)
+    early_segs = (last, last - 1)
+    for seg in early_segs:
+        finish_halo(1, seg)
+        attend_ahead(1, seg, pl.ds(seg * SEG, main))
+    second_keys(last, 0)
+
+    groups = (pl.ds((last - 1) * SEG, 2 * SEG),) + tuple(
+        pl.ds(seg * SEG, SEG) for seg in reversed(range(last - 1))
+    )
+
+    def partner_copy1(g, k):
+        rows = groups[g]
         return send(
-            xsend1.at[k - 1, s],
-            xrecv1.at[k - 1, s],
+            psend1.at[k, rows], precv1.at[k, rows], ps1_sem.at[0], pr_sem.at[g * n_x + k], partner
+        )
+
+    def chip_copy1(g, k):
+        rows = groups[g]
+        return send(
+            xsend1.at[k - 1, rows],
+            xrecv1.at[k - 1, rows],
             xs1_sem.at[k - 1],
-            xr1_sem.at[k - 1, s],
+            xr1_sem.at[k - 1, g],
             peer(k),
         )
 
-    def last_partner(s):
-        for k in range(n_x):
+    far_first = list(range(1, n_x)) + [0]
+
+    def last_partner(g):
+        for k in far_first:
             lower = (chip_at(k) * 2 + 1 - core) * feat
-            psend1[s, k] = project_out(1, lower, feat).astype(BF16)
-        partner_copy1(s).start()
-
-    def last_own(s):
-        for k in range(n_x):
+            psend1[k, groups[g], :] = project_out(1, groups[g], lower, feat).astype(BF16)
+            partner_copy1(g, k).start()
+
+    def last_own(g):
+        for k in far_first:
             lower = (chip_at(k) * 2 + core) * feat
-            own1[s, k] = project_out(1, lower, feat)
-
-    def last_sends(s):
-        partner_copy1(s).wait_recv()
-        for k in range(n_x):
-            both = own1[s, k] + precv1[s, k].astype(F32)
-            if k == 0:
-                own1[s, k] = both
-            else:
-                xsend1[k - 1, s] = both.astype(BF16)
-                chip_copy1(s, k).start()
-
-    attend_rest(1, tail_rows)
+            own1[k, groups[g], :] = project_out(1, groups[g], lower, feat)
+
+    def last_sends(g):
+        for k in range(1, n_x):
+            partner_copy1(g, k).wait_recv()
+            both = own1[k, groups[g], :] + precv1[k, groups[g], :].astype(F32)
+            xsend1[k - 1, groups[g], :] = both.astype(BF16)
+            chip_copy1(g, k).start()
+
+    for seg in early_segs:
+        attend_rest(1, seg, tail_rows)
     last_partner(0)
     second_queries(0)
     last_own(0)
     last_sends(0)
-
-    def last_round(s, carry):
-        finish_halo(1, last - s)
-        attend(1, last - s)
-
-        @pl.when(s > 1)
-        def _():
-            last_sends(s - 1)
-
-        last_partner(s)
-        last_own(s)
-        return carry
-
-    lax.fori_loop(1, segs, last_round, 0)
-    last_sends(last)
+    for g in range(1, len(groups)):
+        finish_halo(1, last - 1 - g)
+        attend(1, last - 1 - g)
+        if g > 1:
+            last_sends(g - 1)
+        last_partner(g)
+        last_own(g)
+    last_sends(len(groups) - 1)
     my_cols = pl.ds(pl.multiple_of(me_tp * feat, 128), feat)
-    for s in range(segs):
-        rows = slice((last - s) * SEG, (segs - s) * SEG)
-        total = own1[s, 0]
+    for g in range(len(groups)):
+        rows = groups[g]
+        partner_copy1(g, 0).wait_recv()
+        total = cur1[rows, my_cols].astype(F32) + own1[0, rows, :] + precv1[0, rows, :].astype(F32)
         for k in range(1, n_x):
-            chip_copy1(s, k).wait_recv()
-            total = total + xrecv1[k - 1, s].astype(F32)
-        out[rows, :] = (cur1[rows, my_cols].astype(F32) + total).astype(BF16)
+            chip_copy1(g, k).wait_recv()
+            total = total + xrecv1[k - 1, rows, :].astype(F32)
+        out[rows, :] = total.astype(BF16)
 
     send(psend, precv, ps_sem.at[0], pr_sem.at[0], partner).wait_send()
     send(cur1.at[:, my_half], cur1.at[:, my_half], cs_sem.at[0], cr_sem.at[0], partner).wait_send()
@@ -527,26 +562,27 @@
         pltpu.VMEM((LAYERS, row_count, 2 * kv_width), BF16),
         pltpu.VMEM((kv_heads, 2 * row_count, 128), BF16),
         pltpu.VMEM((kv_heads, 2 * row_count, 256), BF16),
+        pltpu.VMEM((LAYERS * heads, LINE), F32),
         pltpu.VMEM((LAYERS, segs, heads * SEG, LINE), F32),
-        pltpu.VMEM((kv_heads, group * SEG, 256), F32),
-        pltpu.VMEM((SEG, q_width), BF16),
+        pltpu.VMEM((2, kv_heads, group * SEG, 256), F32),
+        pltpu.VMEM((row_count, q_width), BF16),
         pltpu.VMEM((segs, SEG, half_width), BF16),
         pltpu.VMEM((segs, SEG, half_width), BF16),
         pltpu.VMEM((segs, SEG, half_width), F32),
         pltpu.VMEM((segs, SEG, half_width), BF16),
         pltpu.VMEM((others, segs, SEG, half_width), BF16),
-        pltpu.VMEM((segs, n_x, SEG, feat), BF16),
-        pltpu.VMEM((segs, n_x, SEG, feat), BF16),
-        pltpu.VMEM((segs, n_x, SEG, feat), F32),
-        pltpu.VMEM((others, segs, SEG, feat), BF16),
-        pltpu.VMEM((others, segs, SEG, feat), BF16),
+        pltpu.VMEM((n_x, row_count, feat), BF16),
+        pltpu.VMEM((n_x, row_count, feat), BF16),
+        pltpu.VMEM((n_x, row_count, feat), F32),
+        pltpu.VMEM((others, row_count, feat), BF16),
+        pltpu.VMEM((others, row_count, feat), BF16),
         dma((10,)),
-        dma((1,)), dma((segs,)),
+        dma((1,)), dma((max(segs, (segs - 1) * n_x),)),
         dma((others,)), dma((others, segs)),
         dma((1,)), dma((segs,)),
         dma((LAYERS,)), dma((LAYERS, segs)),
         dma((1,)),
-        dma((others,)), dma((others, segs)),
+        dma((others,)), dma((others, segs - 1)),
     ]
     return pl.pallas_call(
         functools.partial(body, n_sp, n_tp),

time: 37.5 us -> 33.3 us (0.89)
  the two profiles are of different devices: /device:TPU:0 before, /device:TPU:19 now
where the time goes in v2:
time: 33.3 us; the launch traced here: 32.9 us
  Pallas kernels  32.1 us (96%)
  local copies, waits for them, and re-layouts  0.71 us (2%)
    pallas_call x1, Pallas kernels, local(): pl.pallas_call(functools.partial(body, n_sp, n_tp), out_shape=pltpu.VMEM(...  32.1 us
    unnamed x1, local copies, waits for them, and re-layouts  0.71 us

profile of v2, /device:TPU:19, one launch (start us, length us, event | category | flops | bytes accessed | tf_op | source)
XLA Modules:
  0.0 32.9 jit_solution(12437200298156040592)
XLA Ops:
  0.0 32.1 %shard_map.91 = bf16[256,512]{1,0:T(8,128)(2,1)S(1)} custom-call(bf16[256,2048]{1,0:T(8,128)(2,1)} %stream.1, f32[2,2048]{1,0:T(2,128)} %attn_gain_in.1, bf16[2,2048,512]{2,1,0:T(8,128)(2,1)} %w_query.1, bf16[2,2048,128]{2,1,0:T(8,128)(2,1)} %w_key.1, bf16[2,2048,128]{2,1,0:T(8,128)(2,1)} %w_value.1, bf16[2,512,2048]{2,1,0:T(8,128)(2,1)} %w_out.1, ...), custom_call_target="tpu_custom_call" | custom-call | tf_op jit(solution)/shard_map/pallas_call | solution.py:587
  32.2 0.7 %copy.11 = bf16[256,512]{1,0:T(8,128)(2,1)} copy(bf16[256,512]{1,0:T(8,128)(2,1)S(1)} %shard_map.91) | data formatting | bytes 524288

commit v3 on v2

v3 whole, which is shorter than its diff:
```python
import functools

import jax
import jax.numpy as jnp
from jax import lax
from jax.experimental import pallas as pl
from jax.experimental.pallas import tpu as pltpu
from jax.sharding import PartitionSpec as P

HEAD_DIM = 64
SEG = 64
LEFT = 4
CLIP = 128
LAYERS = 2
SPAN = (LEFT + 1) * SEG
LINE = 384
LOG2E = 1.4426950408889634

norm_eps = 1e-06
masked_score = -1e30
F32 = jnp.float32
BF16 = jnp.bfloat16


def seg_rows(seg):
    return pl.ds(pl.multiple_of(seg * SEG, SEG), SEG)


def send(src, dst, send_sem, recv_sem, device):
    return pltpu.make_async_remote_copy(
        src_ref=src,
        dst_ref=dst,
        send_sem=send_sem,
        recv_sem=recv_sem,
        device_id=device,
        device_id_type=pl.DeviceIdType.MESH,
    )


def row_squares(x):
    return jnp.sum(x * x, axis=-1, keepdims=True)


def row_scale(squares, width):
    scale = lax.rsqrt(squares * (1.0 / width) + norm_eps)
    return jnp.broadcast_to(scale, (squares.shape[0], 128))


def widen(scale, width):
    return jnp.concatenate([scale] * -(-width // 128), axis=1)[:, :width]


def head_norm(x, row_scales, gain_row, scale):
    width = x.shape[1]
    x = x * widen(row_scales, width)
    block = min(width, 256)
    row_head = lax.broadcasted_iota(jnp.int32, (block, block), 0) >> 6
    col_head = lax.broadcasted_iota(jnp.int32, (block, block), 1) >> 6
    spread = jnp.where(row_head == col_head, 1.0 / HEAD_DIM, 0.0).astype(BF16)
    gain = jnp.concatenate([gain_row] * (block // HEAD_DIM), axis=1) * scale
    outs = []
    for lower in range(0, width, block):
        part = x[:, lower : lower + block]
        mean = jnp.dot((part * part).astype(BF16), spread, preferred_element_type=F32)
        outs.append((part * lax.rsqrt(mean + norm_eps) * gain).astype(BF16))
    return outs[0] if len(outs) == 1 else jnp.concatenate(outs, axis=1)


def body(
    n_sp, n_tp,
    stream, attn_gain_in, w_query, w_key, w_value, w_out, query_gain_in, key_gain_in, rel_bias_in,
    out,
    attn_gain, query_gain, key_gain, rel_bias,
    cur0, cur1, gained, scales, wq, wkv, wo, queries, pair_made, halo, kdup, vdup, line, bias, ahead, mixed,
    psend, precv, own0, xsend, xrecv,
    psend1, precv1, own1, xsend1, xrecv1,
    w_sem, ps_sem, pr_sem, xs_sem, xr_sem, cs_sem, cr_sem, hs_sem, hr_sem,
    ps1_sem, xs1_sem, xr1_sem,
):
    row_count, width = cur0.shape
    segs = row_count // SEG
    q_width = wq.shape[2]
    kv_width = w_key.shape[2]
    heads = q_width // HEAD_DIM
    kv_heads = kv_width // HEAD_DIM
    group = heads // kv_heads
    n_x = n_tp // 2
    feat = width // n_tp
    half_width = width // 2
    last = segs - 1
    me_sp = lax.axis_index("sp")
    me_tp = lax.axis_index("tp")
    core = lax.rem(me_tp, 2)
    chip = lax.div(me_tp, 2)
    partner = {"tp": chip * 2 + 1 - core}

    def chip_at(k):
        return lax.rem(chip + k, n_x)

    def core_at(k):
        return lax.rem(core + k, 2)

    def peer(k):
        return {"tp": chip_at(k) * 2 + core_at(k)}

    my_part = lax.rem(core + chip, 2)

    barrier = pltpu.get_barrier_semaphore()
    pl.semaphore_signal(barrier, inc=1, device_id=partner, device_id_type=pl.DeviceIdType.MESH)
    for k in range(1, n_x):
        pl.semaphore_signal(barrier, inc=1, device_id=peer(k), device_id_type=pl.DeviceIdType.MESH)

    @pl.when(me_sp > 0)
    def _():
        pl.semaphore_signal(
            barrier, inc=1, device_id={"sp": me_sp - 1}, device_id_type=pl.DeviceIdType.MESH
        )

    @pl.when(me_sp < n_sp - 1)
    def _():
        pl.semaphore_signal(
            barrier, inc=1, device_id={"sp": me_sp + 1}, device_id_type=pl.DeviceIdType.MESH
        )

    def load(n, src, dst):
        copy = pltpu.make_async_copy(src, dst, w_sem.at[n])
        copy.start()
        return copy

    early = pl.ds(last * SEG, SEG)
    late = pl.ds(0, last * SEG)
    early_load = load(0, stream.at[early], cur0.at[early])
    attn_gain_load = load(1, attn_gain_in, attn_gain)
    joined = kv_width % 128 == 0

    def kv_part(l, n):
        if joined:
            return wkv.at[l, :, pl.ds(n * kv_width, kv_width)]
        return wkv.at[l, n]

    wk_load = load(2, w_key.at[0], kv_part(0, 0))
    wv_load = load(3, w_value.at[0], kv_part(0, 1))
    key_gain_load = load(4, key_gain_in, key_gain)
    late_load = load(5, stream.at[late], cur0.at[late])
    rel_bias_load = load(6, rel_bias_in, rel_bias)
    query_gain_load = load(7, query_gain_in, query_gain)
    wq_load = load(8, w_query.at[0], wq.at[0])
    wo_load = load(9, w_out.at[0], wo.at[0])

    low_half = lax.broadcasted_iota(jnp.int32, (SEG, 128), 1) < HEAD_DIM

    def build_line():
        offset = lax.broadcasted_iota(jnp.int32, (2 * CLIP, LINE), 1)
        distance = jnp.clip(LEFT * SEG + SEG - 1 - offset, -CLIP, CLIP) + CLIP
        match = lax.broadcasted_iota(jnp.int32, (2 * CLIP, LINE), 0) == distance
        onehot = jnp.where(match, 1.0, 0.0).astype(BF16)
        far = (distance[:1] == 2 * CLIP).astype(F32)
        table = jnp.concatenate([rel_bias[l] for l in range(LAYERS)], axis=0)
        near = table[:, : 2 * CLIP]
        high = near.astype(BF16)
        near = near - high.astype(F32)
        middle = near.astype(BF16)
        low = (near - middle.astype(F32)).astype(BF16)
        high, middle, low = (
            jnp.dot(part, onehot, preferred_element_type=F32) for part in (high, middle, low)
        )
        line[...] = (high + middle + low + table[:, 2 * CLIP :] * far) * LOG2E

    def build_bias(l):
        for h in range(heads):
            row = slice(l * heads + h, l * heads + h + 1)
            spread = jnp.broadcast_to(line[row, 128:], (SEG, LINE - 128))
            turned = pltpu.roll(spread, LINE - 128 - (SEG - 1), 1, stride=1, stride_axis=0)
            tiles = [
                jnp.broadcast_to(line[row, :128], (SEG, 128)),
                turned[:, :128],
                jnp.where(low_half, turned[:, 128:], masked_score),
            ]
            top = jnp.maximum(jnp.maximum(tiles[0], tiles[1]), tiles[2])
            peak = jnp.max(top, axis=-1, keepdims=True)
            for n in range(3):
                bias[l, 2, h * SEG : (h + 1) * SEG, n * 128 : (n + 1) * 128] = tiles[n] - peak

    def build_edge(l):
        @pl.when(me_sp == 0)
        def _():
            for h in range(heads):
                rows = slice(h * SEG, (h + 1) * SEG)
                near = bias[l, 2, rows, 256:]
                middle = jnp.where(low_half, masked_score, bias[l, 2, rows, 128:256])
                shut = jnp.full((SEG, 128), masked_score, F32)
                peak = jnp.max(near, axis=-1, keepdims=True)
                bias[l, 0, rows, :128] = shut
                bias[l, 0, rows, 128:256] = shut
                bias[l, 0, rows, 256:] = near - peak
                peak = jnp.maximum(peak, jnp.max(middle, axis=-1, keepdims=True))
                bias[l, 1, rows, :128] = shut
                bias[l, 1, rows, 128:256] = middle - peak
                bias[l, 1, rows, 256:] = near - peak

    for kv in range(kv_heads):
        vdup[kv, :, 128:] = jnp.ones((2 * row_count, 128), BF16)

    def take_rows(l, current, rows):
        x = current[rows, :].astype(F32)
        gained[rows, :] = (x * attn_gain[l : l + 1]).astype(BF16)
        scales[rows, :] = row_scale(row_squares(x), width)

    halves = [pl.ds(n * half_width, half_width) for n in range(2)]

    def half_dot(l, rows, half):
        if joined:
            both = wkv[l, half, :]
        else:
            both = jnp.concatenate([wkv[l, 0, half, :], wkv[l, 1, half, :]], axis=1)
        return jnp.dot(gained[rows, half], both, preferred_element_type=F32)

    def keys_values(l, rows):
        flat = half_dot(l, rows, halves[0]) + half_dot(l, rows, halves[1])
        return split_keys(l, rows, flat)

    def split_keys(l, rows, flat):
        keys = head_norm(flat[:, :kv_width], scales[rows, :], key_gain[l : l + 1], 1.0)
        values = flat[:, kv_width:] * widen(scales[rows, :], kv_width)
        return keys, values.astype(BF16)

    def make_queries(l, rows):
        flat = jnp.dot(gained[rows, :], wq[l], preferred_element_type=F32)
        queries[rows, :] = head_norm(
            flat, scales[rows, :], query_gain[l : l + 1], HEAD_DIM ** (-0.5) * LOG2E
        )

    def put_dup(keys, values, rows):
        for kv in range(kv_heads):
            cols = slice(kv * HEAD_DIM, (kv + 1) * HEAD_DIM)
            kdup[kv, rows, :] = jnp.concatenate([keys[:, cols]] * 2, axis=1)
            vdup[kv, rows, :128] = jnp.concatenate([values[:, cols]] * 2, axis=1)

    def halo_copy(l, rows, n):
        return send(
            pair_made.at[l, rows],
            halo.at[l, rows],
            hs_sem.at[l],
            hr_sem.at[n],
            {"sp": lax.rem(me_sp + 1, n_sp)},
        )

    def start_halo(l, rows, n, here=True):
        @pl.when(jnp.logical_and(me_sp < n_sp - 1, here))
        def _():
            halo_copy(l, rows, n).start()

    def finish_halo(l, rows, n):
        @pl.when(me_sp > 0)
        def _():
            halo_copy(l, rows, n).wait_recv()
            got = halo[l, rows, :]
            put_dup(got[:, :kv_width], got[:, kv_width:], rows)

    @pl.when(me_sp == 0)
    def _():
        none = jnp.zeros((row_count, 256), BF16)
        for kv in range(kv_heads):
            kdup[kv, 0:row_count, :] = none[:, :128]
            vdup[kv, 0:row_count, :] = none

    def attend_part(l, seg, kv, rows_at, lanes):
        rows = seg_rows(seg)
        stack = []
        for p in range(group // 2):
            lower = (kv * group + 2 * p) * HEAD_DIM
            tile = queries[rows, lower : lower + 128]
            none = jnp.zeros_like(tile)
            stack += [jnp.where(low_half, tile, none), jnp.where(low_half, none, tile)]
        stacked = jnp.concatenate(stack, axis=0)
        scores = lax.dot_general(
            stacked, kdup[kv, rows_at, :], (((1,), (1,)), ((), ())), preferred_element_type=F32
        )
        base = kv * group * SEG
        table = jnp.where(me_sp == 0, jnp.minimum(seg, 2), 2)
        expon = jnp.exp2(scores + bias[l, table, base : base + group * SEG, lanes]).astype(BF16)
        return jnp.dot(expon, vdup[kv, rows_at, :], preferred_element_type=F32)

    def put_mixed(seg, kv, summed):
        rows = seg_rows(seg)
        for p in range(group // 2):
            lower = (kv * group + 2 * p) * HEAD_DIM
            even = summed[2 * p * SEG : (2 * p + 1) * SEG]
            odd = summed[(2 * p + 1) * SEG : (2 * p + 2) * SEG]
            top = jnp.where(low_half, even[:, :128], odd[:, :128])
            under = jnp.where(low_half, even[:, 128:], odd[:, 128:])
            mixed[rows, lower : lower + 128] = (top / under).astype(BF16)

    def attend(l, seg):
        window = pl.ds(pl.multiple_of(seg * SEG, SEG), SPAN)
        for kv in range(kv_heads):
            put_mixed(seg, kv, attend_part(l, seg, kv, window, slice(0, SPAN)))

    late_keys = pl.ds(last * SEG, 2 * SEG)
    early_keys = pl.ds((last + 2) * SEG, SPAN - 2 * SEG)

    def attend_ahead(l):
        for kv in range(kv_heads):
            ahead[kv] = attend_part(l, last, kv, early_keys, slice(2 * SEG, SPAN))

    def attend_rest(l):
        for kv in range(kv_heads):
            rest = attend_part(l, last, kv, late_keys, slice(0, 2 * SEG))
            put_mixed(last, kv, ahead[kv] + rest)

    def project_out(l, rows, lower, size):
        cols = pl.ds(pl.multiple_of(lower, 128), size)
        return jnp.dot(mixed[rows, :], wo[l, :, cols], preferred_element_type=F32)

    def meet():
        at_edge = jnp.logical_or(me_sp == 0, me_sp == n_sp - 1)

        @pl.when(at_edge)
        def _():
            pl.semaphore_wait(barrier, n_x + min(n_sp - 1, 1))

        @pl.when(jnp.logical_not(at_edge))
        def _():
            pl.semaphore_wait(barrier, n_x + 2)

    early_load.wait()
    attn_gain_load.wait()
    take_rows(0, cur0, early)
    wk_load.wait()
    wv_load.wait()
    key_gain_load.wait()
    keys, values = keys_values(0, early)
    pair_made[0, early, :] = jnp.concatenate([keys, values], axis=1)
    meet()
    start_halo(0, early, last, core == 0)
    put_dup(keys, values, pl.ds(row_count + last * SEG, SEG))
    late_load.wait()
    take_rows(0, cur0, late)
    start_halo(0, early, last, core == 1)
    rel_bias_load.wait()
    build_line()
    keys, values = keys_values(0, late)
    pair_made[0, late, :] = jnp.concatenate([keys, values], axis=1)
    start_halo(0, late, 0)
    put_dup(keys, values, pl.ds(row_count, last * SEG))
    query_gain_load.wait()
    wq_load.wait()
    make_queries(0, early)
    build_bias(0)
    out_step = min(half_width, 512)
    whole_piece = pl.ds(0, half_width)
    first_pieces = [pl.ds(lower, out_step) for lower in range(0, half_width, out_step)]

    def pieces_of(i):
        if isinstance(i, int) and i == 0:
            return [(0 if n == 0 else segs + n - 1, cols) for n, cols in enumerate(first_pieces)]
        return [(i, whole_piece)]

    def partner_copy(i, n, cols):
        return send(
            psend.at[i, :, cols], precv.at[i, :, cols], ps_sem.at[0], pr_sem.at[n], partner
        )

    def chip_copy(i, k, n, cols):
        return send(
            xsend.at[i, :, cols],
            xrecv.at[k - 1, i, :, cols],
            xs_sem.at[k - 1],
            xr_sem.at[k - 1, n],
            peer(k),
        )

    my_half = pl.ds(pl.multiple_of(my_part * half_width, 128), half_width)

    def rows_copy(i, seg):
        rows = seg_rows(seg)
        return send(
            cur1.at[rows, my_half], cur1.at[rows, my_half], cs_sem.at[0], cr_sem.at[i], partner
        )

    def first_partner(i):
        for n, cols in pieces_of(i):
            for lower in range(cols.start, cols.start + cols.size, out_step):
                psend[i, :, lower : lower + out_step] = project_out(
                    0, seg_rows(last - i), (1 - my_part) * half_width + lower, out_step
                ).astype(BF16)
            partner_copy(i, n, cols).start()

    def first_own(i):
        for lower in range(0, half_width, out_step):
            own0[i, :, lower : lower + out_step] = project_out(
                0, seg_rows(last - i), my_part * half_width + lower, out_step
            )

    def first_sends(i):
        for n, cols in pieces_of(i):
            partner_copy(i, n, cols).wait_recv()
            both = own0[i, :, cols] + precv[i, :, cols].astype(F32)
            own0[i, :, cols] = both
            xsend[i, :, cols] = both.astype(BF16)
            for k in range(1, n_x):
                chip_copy(i, k, n, cols).start()

    attend_ahead(0)
    finish_halo(0, early, last)
    wo_load.wait()
    attend_rest(0)
    first_partner(0)
    first_own(0)
    first_sends(0)
    make_queries(0, seg_rows(last - 1))
    second_loads = [
        load(2, w_key.at[1], kv_part(1, 0)),
        load(3, w_value.at[1], kv_part(1, 1)),
        load(8, w_query.at[1], wq.at[1]),
        load(9, w_out.at[1], wo.at[1]),
    ]
    finish_halo(0, late, 0)
    attend(0, last - 1)
    first_partner(1)
    first_own(1)
    make_queries(0, pl.ds(0, (last - 1) * SEG))
    build_edge(0)
    first_sends(1)

    def first_round(i, carry):
        attend(0, last - i)
        first_partner(i)

        @pl.when(i > 2)
        def _():
            first_sends(i - 1)

        first_own(i)
        return carry

    lax.fori_loop(2, segs, first_round, 0)
    first_sends(last)

    def gather_rows(i, seg):
        rows = seg_rows(seg)
        total = own0[i]
        for k in range(1, n_x):
            for n, cols in pieces_of(i):
                chip_copy(i, k, n, cols).wait_recv()
            total = total + xrecv[k - 1, i].astype(F32)
        mine = (cur0[rows, my_half].astype(F32) + total).astype(BF16)
        cur1[rows, my_half] = mine
        rows_copy(i, seg).start()
        return half_rows(seg, my_half)

    def half_rows(seg, half):
        rows = seg_rows(seg)
        x = cur1[rows, half].astype(F32)
        gained[rows, half] = (x * attn_gain[1:2, half]).astype(BF16)
        return row_squares(x), half_dot(1, rows, half)

    their_half = pl.ds(pl.multiple_of((1 - my_part) * half_width, 128), half_width)

    def second_keys(i, seg, squares, flat):
        rows = seg_rows(seg)
        rows_copy(i, seg).wait_recv()
        more_squares, more_flat = half_rows(seg, their_half)
        scales[rows, :] = row_scale(squares + more_squares, width)
        keys, values = split_keys(1, rows, flat + more_flat)
        pair_made[1, rows, :] = jnp.concatenate([keys, values], axis=1)
        start_halo(1, rows, segs + seg)
        put_dup(keys, values, pl.ds(pl.multiple_of(row_count + seg * SEG, SEG), SEG))

    for copy in second_loads:
        copy.wait()
    begun = gather_rows(0, last)
    build_bias(1)
    build_edge(1)
    second_keys(0, last, *begun)

    def second_round(i, carry):
        begun = gather_rows(i, last - i)
        make_queries(1, seg_rows(segs - i))
        second_keys(i, last - i, *begun)
        return carry

    lax.fori_loop(1, last, second_round, 0)
    begun = gather_rows(last, 0)
    make_queries(1, seg_rows(1))
    attend_ahead(1)
    finish_halo(1, seg_rows(last), segs + last)
    second_keys(last, 0, *begun)

    groups = tuple(pl.ds(seg * SEG, SEG) for seg in reversed(range(segs)))

    def partner_copy1(g, k):
        rows = groups[g]
        return send(
            psend1.at[k, rows], precv1.at[k, rows], ps1_sem.at[0], pr_sem.at[g * n_x + k], partner
        )

    def chip_copy1(g, k):
        rows = groups[g]
        return send(
            xsend1.at[k - 1, rows],
            xrecv1.at[k - 1, rows],
            xs1_sem.at[k - 1],
            xr1_sem.at[k - 1, g],
            peer(k),
        )

    far = range(1, n_x)

    def last_partner(g, which):
        for k in which:
            lower = (chip_at(k) * 2 + 1 - core_at(k)) * feat
            psend1[k, groups[g], :] = project_out(1, groups[g], lower, feat).astype(BF16)
            partner_copy1(g, k).start()

    def last_own(g, which):
        for k in which:
            lower = (chip_at(k) * 2 + core_at(k)) * feat
            own1[k, groups[g], :] = project_out(1, groups[g], lower, feat)

    def last_sends(g):
        for k in far:
            partner_copy1(g, k).wait_recv()
            both = own1[k, groups[g], :] + precv1[k, groups[g], :].astype(F32)
            xsend1[k - 1, groups[g], :] = both.astype(BF16)
            chip_copy1(g, k).start()

    attend_rest(1)
    last_partner(0, far)
    for g in range(1, segs):
        if g == last:
            make_queries(1, seg_rows(0))
            last_own(g - 1, far)
            last_sends(g - 1)
        finish_halo(1, seg_rows(last - g), segs + last - g)
        attend(1, last - g)
        if g < last:
            last_own(g - 1, far)
            last_partner(g - 1, [0])
            last_sends(g - 1)
        last_partner(g, far)
    last_partner(last - 1, [0])
    last_own(last, far)
    last_partner(last, [0])
    last_own(0, [0])
    last_sends(last)
    for g in range(1, segs):
        last_own(g, [0])
    my_cols = pl.ds(pl.multiple_of(me_tp * feat, 128), feat)
    for g in range(len(groups)):
        rows = groups[g]
        partner_copy1(g, 0).wait_recv()
        total = cur1[rows, my_cols].astype(F32) + own1[0, rows, :] + precv1[0, rows, :].astype(F32)
        for k in range(1, n_x):
            chip_copy1(g, k).wait_recv()
            total = total + xrecv1[k - 1, rows, :].astype(F32)
        out[rows, :] = total.astype(BF16)

    send(psend, precv, ps_sem.at[0], pr_sem.at[0], partner).wait_send()
    send(cur1.at[:, my_half], cur1.at[:, my_half], cs_sem.at[0], cr_sem.at[0], partner).wait_send()
    send(psend1, precv1, ps1_sem.at[0], pr_sem.at[0], partner).wait_send()
    for k in range(1, n_x):
        send(xsend, xrecv.at[k - 1], xs_sem.at[k - 1], xr_sem.at[k - 1, 0], peer(k)).wait_send()
        send(
            xsend1.at[k - 1], xrecv1.at[k - 1], xs1_sem.at[k - 1], xr1_sem.at[k - 1, 0], peer(k)
        ).wait_send()

    @pl.when(me_sp < n_sp - 1)
    def _():
        for l in range(LAYERS):
            send(
                pair_made.at[l], halo.at[l], hs_sem.at[l], hr_sem.at[0],
                {"sp": lax.rem(me_sp + 1, n_sp)},
            ).wait_send()


def local(n_sp, n_tp, stream, attn_gain, w_query, w_key, w_value, w_out, query_gain, key_gain, rel_bias):
    row_count, width = stream.shape
    segs = row_count // SEG
    assert row_count == LEFT * SEG and n_tp % 2 == 0
    n_x = n_tp // 2
    feat = width // n_tp
    half_width = width // 2
    q_width = w_query.shape[2]
    kv_width = w_key.shape[2]
    kv_heads = kv_width // HEAD_DIM
    heads = q_width // HEAD_DIM
    group = heads // kv_heads
    others = max(n_x - 1, 1)
    dma = pltpu.SemaphoreType.DMA
    anyw = pl.BlockSpec(memory_space=pltpu.HBM)
    vmem = pl.BlockSpec(memory_space=pltpu.VMEM)
    scratch = [
        pltpu.VMEM(attn_gain.shape, F32),
        pltpu.VMEM(query_gain.shape, F32),
        pltpu.VMEM(key_gain.shape, F32),
        pltpu.VMEM(rel_bias.shape, F32),
        pltpu.VMEM((row_count, width), BF16),
        pltpu.VMEM((row_count, width), BF16),
        pltpu.VMEM((row_count, width), BF16),
        pltpu.VMEM((row_count, 128), F32),
        pltpu.VMEM(w_query.shape, BF16),
        pltpu.VMEM(
            (LAYERS, width, 2 * kv_width) if kv_width % 128 == 0 else (LAYERS, 2, width, kv_width),
            BF16,
        ),
        pltpu.VMEM(w_out.shape, BF16),
        pltpu.VMEM((row_count, q_width), BF16),
        pltpu.VMEM((LAYERS, row_count, 2 * kv_width), BF16),
        pltpu.VMEM((LAYERS, row_count, 2 * kv_width), BF16),
        pltpu.VMEM((kv_heads, 2 * row_count, 128), BF16),
        pltpu.VMEM((kv_heads, 2 * row_count, 256), BF16),
        pltpu.VMEM((LAYERS * heads, LINE), F32),
        pltpu.VMEM((LAYERS, 3, heads * SEG, LINE), F32),
        pltpu.VMEM((kv_heads, group * SEG, 256), F32),
        pltpu.VMEM((row_count, q_width), BF16),
        pltpu.VMEM((segs, SEG, half_width), BF16),
        pltpu.VMEM((segs, SEG, half_width), BF16),
        pltpu.VMEM((segs, SEG, half_width), F32),
        pltpu.VMEM((segs, SEG, half_width), BF16),
        pltpu.VMEM((others, segs, SEG, half_width), BF16),
        pltpu.VMEM((n_x, row_count, feat), BF16),
        pltpu.VMEM((n_x, row_count, feat), BF16),
        pltpu.VMEM((n_x, row_count, feat), F32),
        pltpu.VMEM((others, row_count, feat), BF16),
        pltpu.VMEM((others, row_count, feat), BF16),
        dma((10,)),
        dma((1,)), dma((max(segs * n_x, 2 * segs),)),
        dma((others,)), dma((others, segs + half_width // min(half_width, 512) - 1)),
        dma((1,)), dma((segs,)),
        dma((LAYERS,)), dma((LAYERS * segs,)),
        dma((1,)),
        dma((others,)), dma((others, segs)),
    ]
    return pl.pallas_call(
        functools.partial(body, n_sp, n_tp),
        out_shape=pltpu.VMEM((row_count, feat), BF16),
        in_specs=[anyw] * 9,
        out_specs=vmem,
        scratch_shapes=scratch,
        compiler_params=pltpu.CompilerParams(
            collective_id=0, has_side_effects=True, vmem_limit_bytes=60 * 1024 * 1024
        ),
    )(stream, attn_gain, w_query, w_key, w_value, w_out, query_gain, key_gain, rel_bias)


def solution(mesh):
    return jax.shard_map(
        functools.partial(local, mesh.shape["sp"], mesh.shape["tp"]),
        mesh=mesh,
        in_specs=(
            P("sp", None),
            P(),
            P(None, None, "tp"),
            P(None, None, "tp"),
            P(None, None, "tp"),
            P(None, "tp", None),
            P(),
            P(),
            P(None, "tp", None),
        ),
        out_specs=P("sp", "tp"),
        check_vma=False,
    )
```

time: 33.3 us -> 32.3 us (0.970)
  Pallas kernels: 32.1 us -> 31.4 us
    pallas_call x1, Pallas kernels: 32.1 us -> 31.4 us  [local(): pl.pallas_call(functools.partial(body, n_sp, n_tp), out_shape=pltpu.VMEM(...]
where the time goes in v3:
time: 32.3 us; the launch traced here: 32.1 us
  Pallas kernels  31.4 us (97%)
  local copies, waits for them, and re-layouts  0.71 us (2%)
    pallas_call x1, Pallas kernels, local(): pl.pallas_call(functools.partial(body, n_sp, n_tp), out_shape=pltpu.VMEM(...  31.4 us
    unnamed x1, local copies, waits for them, and re-layouts  0.71 us

profile of v3, /device:TPU:19, one launch (start us, length us, event | category | flops | bytes accessed | tf_op | source)
XLA Modules:
  0.0 32.1 jit_solution(15261943784104172953)
XLA Ops:
  0.0 31.4 %shard_map.91 = bf16[256,512]{1,0:T(8,128)(2,1)S(1)} custom-call(bf16[256,2048]{1,0:T(8,128)(2,1)} %stream.1, f32[2,2048]{1,0:T(2,128)} %attn_gain_in.1, bf16[2,2048,512]{2,1,0:T(8,128)(2,1)} %w_query.1, bf16[2,2048,128]{2,1,0:T(8,128)(2,1)} %w_key.1, bf16[2,2048,128]{2,1,0:T(8,128)(2,1)} %w_value.1, bf16[2,512,2048]{2,1,0:T(8,128)(2,1)} %w_out.1, ...), custom_call_target="tpu_custom_call" | custom-call | tf_op jit(solution)/shard_map/pallas_call | solution.py:635
  31.4 0.7 %copy.11 = bf16[256,512]{1,0:T(8,128)(2,1)} copy(bf16[256,512]{1,0:T(8,128)(2,1)S(1)} %shard_map.91) | data formatting | bytes 524288

commit v4 on v3

--- a/solution.py
+++ b/solution.py
@@ -50,9 +50,8 @@
     return jnp.concatenate([scale] * -(-width // 128), axis=1)[:, :width]
 
 
-def head_norm(x, row_scales, gain_row, scale):
+def head_norm(x, gain_row, scale):
     width = x.shape[1]
-    x = x * widen(row_scales, width)
     block = min(width, 256)
     row_head = lax.broadcasted_iota(jnp.int32, (block, block), 0) >> 6
     col_head = lax.broadcasted_iota(jnp.int32, (block, block), 1) >> 6
@@ -74,8 +73,7 @@
     cur0, cur1, gained, scales, wq, wkv, wo, queries, pair_made, halo, kdup, vdup, line, bias, ahead, mixed,
     psend, precv, own0, xsend, xrecv,
     psend1, precv1, own1, xsend1, xrecv1,
-    w_sem, ps_sem, pr_sem, xs_sem, xr_sem, cs_sem, cr_sem, hs_sem, hr_sem,
-    ps1_sem, xs1_sem, xr1_sem,
+    w_sem, ps_sem, pr_sem, xs_sem, xr_sem, cr_sem, hs_sem, hr_sem, xr1_sem,
 ):
     row_count, width = cur0.shape
     segs = row_count // SEG
@@ -129,7 +127,9 @@
 
     early = pl.ds(last * SEG, SEG)
     late = pl.ds(0, last * SEG)
-    early_load = load(0, stream.at[early], cur0.at[early])
+    for lower in range(last * SEG, row_count, 16):
+        load(0, stream.at[pl.ds(lower, 16)], cur0.at[pl.ds(lower, 16)])
+    early_load = pltpu.make_async_copy(stream.at[early], cur0.at[early], w_sem.at[0])
     attn_gain_load = load(1, attn_gain_in, attn_gain)
     joined = kv_width % 128 == 0
 
@@ -216,18 +216,20 @@
         return jnp.dot(gained[rows, half], both, preferred_element_type=F32)
 
     def keys_values(l, rows):
-        flat = half_dot(l, rows, halves[0]) + half_dot(l, rows, halves[1])
-        return split_keys(l, rows, flat)
-
-    def split_keys(l, rows, flat):
-        keys = head_norm(flat[:, :kv_width], scales[rows, :], key_gain[l : l + 1], 1.0)
-        values = flat[:, kv_width:] * widen(scales[rows, :], kv_width)
-        return keys, values.astype(BF16)
+        row_scales = widen(scales[rows, :], 2 * kv_width)
+        flat = half_dot(l, rows, halves[0]) * row_scales + half_dot(l, rows, halves[1]) * row_scales
+        return split_keys(l, flat)
+
+    def split_keys(l, flat):
+        keys = head_norm(flat[:, :kv_width], key_gain[l : l + 1], 1.0)
+        return keys, flat[:, kv_width:].astype(BF16)
 
     def make_queries(l, rows):
         flat = jnp.dot(gained[rows, :], wq[l], preferred_element_type=F32)
         queries[rows, :] = head_norm(
-            flat, scales[rows, :], query_gain[l : l + 1], HEAD_DIM ** (-0.5) * LOG2E
+            flat * widen(scales[rows, :], q_width),
+            query_gain[l : l + 1],
+            HEAD_DIM ** (-0.5) * LOG2E,
         )
 
     def put_dup(keys, values, rows):
@@ -240,7 +242,7 @@
         return send(
             pair_made.at[l, rows],
             halo.at[l, rows],
-            hs_sem.at[l],
+            hs_sem.at[0],
             hr_sem.at[n],
             {"sp": lax.rem(me_sp + 1, n_sp)},
         )
@@ -249,6 +251,14 @@
         @pl.when(jnp.logical_and(me_sp < n_sp - 1, here))
         def _():
             halo_copy(l, rows, n).start()
+
+    def end_halo(l):
+        @pl.when(me_sp < n_sp - 1)
+        def _():
+            send(
+                pair_made.at[l], halo.at[l], hs_sem.at[0], hr_sem.at[0],
+                {"sp": lax.rem(me_sp + 1, n_sp)},
+            ).wait_send()
 
     def finish_halo(l, rows, n):
         @pl.when(me_sp > 0)
@@ -332,11 +342,11 @@
     keys, values = keys_values(0, early)
     pair_made[0, early, :] = jnp.concatenate([keys, values], axis=1)
     meet()
-    start_halo(0, early, last, core == 0)
+    start_halo(0, early, 1, core == 0)
     put_dup(keys, values, pl.ds(row_count + last * SEG, SEG))
     late_load.wait()
     take_rows(0, cur0, late)
-    start_halo(0, early, last, core == 1)
+    start_halo(0, early, 1, core == 1)
     rel_bias_load.wait()
     build_line()
     keys, values = keys_values(0, late)
@@ -375,7 +385,7 @@
     def rows_copy(i, seg):
         rows = seg_rows(seg)
         return send(
-            cur1.at[rows, my_half], cur1.at[rows, my_half], cs_sem.at[0], cr_sem.at[i], partner
+            cur1.at[rows, my_half], cur1.at[rows, my_half], ps_sem.at[0], cr_sem.at[i], partner
         )
 
     def first_partner(i):
@@ -402,7 +412,7 @@
                 chip_copy(i, k, n, cols).start()
 
     attend_ahead(0)
-    finish_halo(0, early, last)
+    finish_halo(0, early, 1)
     wo_load.wait()
     attend_rest(0)
     first_partner(0)
@@ -447,31 +457,43 @@
         mine = (cur0[rows, my_half].astype(F32) + total).astype(BF16)
         cur1[rows, my_half] = mine
         rows_copy(i, seg).start()
-        return half_rows(seg, my_half)
+        squares = half_rows(seg, my_half)
+        return squares, half_dot(1, rows, my_half)
 
     def half_rows(seg, half):
         rows = seg_rows(seg)
         x = cur1[rows, half].astype(F32)
         gained[rows, half] = (x * attn_gain[1:2, half]).astype(BF16)
-        return row_squares(x), half_dot(1, rows, half)
-
-    their_half = pl.ds(pl.multiple_of((1 - my_part) * half_width, 128), half_width)
+        return row_squares(x)
+
+    their_start = (1 - my_part) * half_width
+    their_half = pl.ds(pl.multiple_of(their_start, 128), half_width)
+    quarters = [
+        pl.ds(pl.multiple_of(their_start + n * (half_width // 2), 128), half_width // 2)
+        for n in range(2)
+    ]
 
     def second_keys(i, seg, squares, flat):
         rows = seg_rows(seg)
         rows_copy(i, seg).wait_recv()
-        more_squares, more_flat = half_rows(seg, their_half)
-        scales[rows, :] = row_scale(squares + more_squares, width)
-        keys, values = split_keys(1, rows, flat + more_flat)
+        row_scales = row_scale(squares + half_rows(seg, their_half), width)
+        scales[rows, :] = row_scales
+        row_scales = widen(row_scales, 2 * kv_width)
+        flat = flat * row_scales
+        for part in quarters:
+            flat = flat + half_dot(1, rows, part) * row_scales
+        keys, values = split_keys(1, flat)
         pair_made[1, rows, :] = jnp.concatenate([keys, values], axis=1)
-        start_halo(1, rows, segs + seg)
+        start_halo(1, rows, 2 + seg)
         put_dup(keys, values, pl.ds(pl.multiple_of(row_count + seg * SEG, SEG), SEG))
 
+    send(psend, precv, ps_sem.at[0], pr_sem.at[0], partner).wait_send()
     for copy in second_loads:
         copy.wait()
     begun = gather_rows(0, last)
     build_bias(1)
     build_edge(1)
+    end_halo(0)
     second_keys(0, last, *begun)
 
     def second_round(i, carry):
@@ -484,15 +506,18 @@
     begun = gather_rows(last, 0)
     make_queries(1, seg_rows(1))
     attend_ahead(1)
-    finish_halo(1, seg_rows(last), segs + last)
+    finish_halo(1, seg_rows(last), 2 + last)
     second_keys(last, 0, *begun)
 
     groups = tuple(pl.ds(seg * SEG, SEG) for seg in reversed(range(segs)))
+
+    def near(g, k):
+        return segs if k == 0 else (g if k == 1 else segs + 1 + (k - 2) * segs + g)
 
     def partner_copy1(g, k):
         rows = groups[g]
         return send(
-            psend1.at[k, rows], precv1.at[k, rows], ps1_sem.at[0], pr_sem.at[g * n_x + k], partner
+            psend1.at[k, rows], precv1.at[k, rows], ps_sem.at[0], pr_sem.at[near(g, k)], partner
         )
 
     def chip_copy1(g, k):
@@ -500,7 +525,7 @@
         return send(
             xsend1.at[k - 1, rows],
             xrecv1.at[k - 1, rows],
-            xs1_sem.at[k - 1],
+            xs_sem.at[k - 1],
             xr1_sem.at[k - 1, g],
             peer(k),
         )
@@ -525,6 +550,10 @@
             xsend1[k - 1, groups[g], :] = both.astype(BF16)
             chip_copy1(g, k).start()
 
+    rows_sent = cur1.at[:, my_half]
+    send(rows_sent, rows_sent, ps_sem.at[0], cr_sem.at[0], partner).wait_send()
+    for k in far:
+        send(xsend, xrecv.at[k - 1], xs_sem.at[k - 1], xr_sem.at[k - 1, 0], peer(k)).wait_send()
     attend_rest(1)
     last_partner(0, far)
     for g in range(1, segs):
@@ -532,7 +561,7 @@
             make_queries(1, seg_rows(0))
             last_own(g - 1, far)
             last_sends(g - 1)
-        finish_halo(1, seg_rows(last - g), segs + last - g)
+        finish_halo(1, seg_rows(last - g), 2 + last - g)
         attend(1, last - g)
         if g < last:
             last_own(g - 1, far)
@@ -547,31 +576,21 @@
     for g in range(1, segs):
         last_own(g, [0])
     my_cols = pl.ds(pl.multiple_of(me_tp * feat, 128), feat)
+    send(psend1.at[0], precv1.at[0], ps_sem.at[0], pr_sem.at[segs], partner).wait_recv()
     for g in range(len(groups)):
         rows = groups[g]
-        partner_copy1(g, 0).wait_recv()
         total = cur1[rows, my_cols].astype(F32) + own1[0, rows, :] + precv1[0, rows, :].astype(F32)
         for k in range(1, n_x):
             chip_copy1(g, k).wait_recv()
             total = total + xrecv1[k - 1, rows, :].astype(F32)
         out[rows, :] = total.astype(BF16)
 
-    send(psend, precv, ps_sem.at[0], pr_sem.at[0], partner).wait_send()
-    send(cur1.at[:, my_half], cur1.at[:, my_half], cs_sem.at[0], cr_sem.at[0], partner).wait_send()
-    send(psend1, precv1, ps1_sem.at[0], pr_sem.at[0], partner).wait_send()
+    send(psend1, precv1, ps_sem.at[0], pr_sem.at[0], partner).wait_send()
     for k in range(1, n_x):
-        send(xsend, xrecv.at[k - 1], xs_sem.at[k - 1], xr_sem.at[k - 1, 0], peer(k)).wait_send()
         send(
-            xsend1.at[k - 1], xrecv1.at[k - 1], xs1_sem.at[k - 1], xr1_sem.at[k - 1, 0], peer(k)
+            xsend1.at[k - 1], xrecv1.at[k - 1], xs_sem.at[k - 1], xr1_sem.at[k - 1, 0], peer(k)
         ).wait_send()
-
-    @pl.when(me_sp < n_sp - 1)
-    def _():
-        for l in range(LAYERS):
-            send(
-                pair_made.at[l], halo.at[l], hs_sem.at[l], hr_sem.at[0],
-                {"sp": lax.rem(me_sp + 1, n_sp)},
-            ).wait_send()
+    end_halo(1)
 
 
 def local(n_sp, n_tp, stream, attn_gain, w_query, w_key, w_value, w_out, query_gain, key_gain, rel_bias):
@@ -625,12 +644,11 @@
         pltpu.VMEM((others, row_count, feat), BF16),
         pltpu.VMEM((others, row_count, feat), BF16),
         dma((10,)),
-        dma((1,)), dma((max(segs * n_x, 2 * segs),)),
+        dma((1,)), dma((segs + 1 + (others - 1) * segs,)),
         dma((others,)), dma((others, segs + half_width // min(half_width, 512) - 1)),
-        dma((1,)), dma((segs,)),
-        dma((LAYERS,)), dma((LAYERS * segs,)),
-        dma((1,)),
-        dma((others,)), dma((others, segs)),
+        dma((segs,)),
+        dma((1,)), dma((2 + segs,)),
+        dma((others, segs)),
     ]
     return pl.pallas_call(
         functools.partial(body, n_sp, n_tp),

time: 32.3 us -> 32 us (level)
  no operation moved by 1% of the time
where the time goes in v4:
time: 32 us; the launch traced here: 31.9 us
  Pallas kernels  31.2 us (98%)
  local copies, waits for them, and re-layouts  0.71 us (2%)
    pallas_call x1, Pallas kernels, local(): pl.pallas_call(functools.partial(body, n_sp, n_tp), out_shape=pltpu.VMEM(...  31.2 us
    unnamed x1, local copies, waits for them, and re-layouts  0.71 us

profile of v4, /device:TPU:19, one launch (start us, length us, event | category | flops | bytes accessed | tf_op | source)
XLA Modules:
  0.0 31.9 jit_solution(10924991335493214631)
XLA Ops:
  0.0 31.2 %shard_map.91 = bf16[256,512]{1,0:T(8,128)(2,1)S(1)} custom-call(bf16[256,2048]{1,0:T(8,128)(2,1)} %stream.1, f32[2,2048]{1,0:T(2,128)} %attn_gain_in.1, bf16[2,2048,512]{2,1,0:T(8,128)(2,1)} %w_query.1, bf16[2,2048,128]{2,1,0:T(8,128)(2,1)} %w_key.1, bf16[2,2048,128]{2,1,0:T(8,128)(2,1)} %w_value.1, bf16[2,512,2048]{2,1,0:T(8,128)(2,1)} %w_out.1, ...), custom_call_target="tpu_custom_call" | custom-call | tf_op jit(solution)/shard_map/pallas_call | solution.py:653
  31.2 0.7 %copy.11 = bf16[256,512]{1,0:T(8,128)(2,1)} copy(bf16[256,512]{1,0:T(8,128)(2,1)S(1)} %shard_map.91) | data formatting | bytes 524288

commit v5 on v4

--- a/solution.py
+++ b/solution.py
@@ -15,6 +15,7 @@
 SPAN = (LEFT + 1) * SEG
 LINE = 384
 LOG2E = 1.4426950408889634
+DIRECT = 16
 
 norm_eps = 1e-06
 masked_score = -1e30
@@ -72,8 +73,8 @@
     attn_gain, query_gain, key_gain, rel_bias,
     cur0, cur1, gained, scales, wq, wkv, wo, queries, pair_made, halo, kdup, vdup, line, bias, ahead, mixed,
     psend, precv, own0, xsend, xrecv,
-    psend1, precv1, own1, xsend1, xrecv1,
-    w_sem, ps_sem, pr_sem, xs_sem, xr_sem, cr_sem, hs_sem, hr_sem, xr1_sem,
+    psend1, precv1, own1, xsend1, xrecv1, dsend, drecv,
+    w_sem, ps_sem, pr_sem, xs_sem, xr_sem, cr_sem, hs_sem, hr_sem, xr1_sem, ds_sem, dr_sem,
 ):
     row_count, width = cur0.shape
     segs = row_count // SEG
@@ -101,12 +102,16 @@
     def peer(k):
         return {"tp": chip_at(k) * 2 + core_at(k)}
 
+    def far_peer(k):
+        return {"tp": chip_at(k) * 2 + 1 - core_at(k)}
+
     my_part = lax.rem(core + chip, 2)
 
     barrier = pltpu.get_barrier_semaphore()
     pl.semaphore_signal(barrier, inc=1, device_id=partner, device_id_type=pl.DeviceIdType.MESH)
     for k in range(1, n_x):
-        pl.semaphore_signal(barrier, inc=1, device_id=peer(k), device_id_type=pl.DeviceIdType.MESH)
+        for there in (peer(k), far_peer(k)):
+            pl.semaphore_signal(barrier, inc=1, device_id=there, device_id_type=pl.DeviceIdType.MESH)
 
     @pl.when(me_sp > 0)
     def _():
@@ -327,11 +332,11 @@
 
         @pl.when(at_edge)
         def _():
-            pl.semaphore_wait(barrier, n_x + min(n_sp - 1, 1))
+            pl.semaphore_wait(barrier, 2 * n_x - 1 + min(n_sp - 1, 1))
 
         @pl.when(jnp.logical_not(at_edge))
         def _():
-            pl.semaphore_wait(barrier, n_x + 2)
+            pl.semaphore_wait(barrier, 2 * n_x - 1 + 2)
 
     early_load.wait()
     attn_gain_load.wait()
@@ -512,16 +517,20 @@
     groups = tuple(pl.ds(seg * SEG, SEG) for seg in reversed(range(segs)))
 
     def near(g, k):
-        return segs if k == 0 else (g if k == 1 else segs + 1 + (k - 2) * segs + g)
+        return g if k == 1 else segs + 1 + (k - 2) * segs + g
+
+    head = last * SEG
+    summed_rows = (pl.ds(head + DIRECT, SEG - DIRECT),) + groups[1:]
+    beyond = pl.ds(DIRECT, row_count - DIRECT)
 
     def partner_copy1(g, k):
-        rows = groups[g]
+        rows = summed_rows[g]
         return send(
-            psend1.at[k, rows], precv1.at[k, rows], ps_sem.at[0], pr_sem.at[near(g, k)], partner
+            psend1.at[k, rows], precv1.at[k, rows], ps_sem.at[k], pr_sem.at[near(g, k)], partner
         )
 
     def chip_copy1(g, k):
-        rows = groups[g]
+        rows = summed_rows[g]
         return send(
             xsend1.at[k - 1, rows],
             xrecv1.at[k - 1, rows],
@@ -530,24 +539,42 @@
             peer(k),
         )
 
+    def direct_copy(k, n):
+        return send(
+            dsend.at[k - 1, n],
+            drecv.at[k - 1, n],
+            ds_sem.at[k - 1],
+            dr_sem.at[k - 1, n],
+            peer(k) if n else far_peer(k),
+        )
+
     far = range(1, n_x)
 
     def last_partner(g, which):
         for k in which:
             lower = (chip_at(k) * 2 + 1 - core_at(k)) * feat
-            psend1[k, groups[g], :] = project_out(1, groups[g], lower, feat).astype(BF16)
+            made = project_out(1, groups[g], lower, feat).astype(BF16)
+            psend1[k, groups[g], :] = made
+            if g == 0:
+                dsend[k - 1, 0] = made[:DIRECT]
+                direct_copy(k, 0).start()
             partner_copy1(g, k).start()
 
     def last_own(g, which):
         for k in which:
             lower = (chip_at(k) * 2 + core_at(k)) * feat
-            own1[k, groups[g], :] = project_out(1, groups[g], lower, feat)
+            made = project_out(1, groups[g], lower, feat)
+            own1[k, groups[g], :] = made
+            if g == 0:
+                dsend[k - 1, 1] = made[:DIRECT].astype(BF16)
+                direct_copy(k, 1).start()
 
     def last_sends(g):
+        rows = summed_rows[g]
         for k in far:
             partner_copy1(g, k).wait_recv()
-            both = own1[k, groups[g], :] + precv1[k, groups[g], :].astype(F32)
-            xsend1[k - 1, groups[g], :] = both.astype(BF16)
+            both = own1[k, rows, :] + precv1[k, rows, :].astype(F32)
+            xsend1[k - 1, rows, :] = both.astype(BF16)
             chip_copy1(g, k).start()
 
     rows_sent = cur1.at[:, my_half]
@@ -556,39 +583,62 @@
         send(xsend, xrecv.at[k - 1], xs_sem.at[k - 1], xr_sem.at[k - 1, 0], peer(k)).wait_send()
     attend_rest(1)
     last_partner(0, far)
+    last_own(0, far)
     for g in range(1, segs):
         if g == last:
-            make_queries(1, seg_rows(0))
             last_own(g - 1, far)
-            last_sends(g - 1)
         finish_halo(1, seg_rows(last - g), 2 + last - g)
         attend(1, last - g)
-        if g < last:
+        if 1 < g < last:
             last_own(g - 1, far)
-            last_partner(g - 1, [0])
-            last_sends(g - 1)
+        if g == last - 1:
+            make_queries(1, seg_rows(0))
+        last_sends(g - 1)
         last_partner(g, far)
-    last_partner(last - 1, [0])
     last_own(last, far)
-    last_partner(last, [0])
-    last_own(0, [0])
     last_sends(last)
-    for g in range(1, segs):
-        last_own(g, [0])
+    near_copy = send(psend1.at[0], precv1.at[0], ps_sem.at[0], pr_sem.at[segs], partner)
+    every = pl.ds(0, row_count)
+    psend1[0] = project_out(1, every, (chip * 2 + 1 - core) * feat, feat).astype(BF16)
+    near_copy.start()
+    own1[0] = project_out(1, every, (chip * 2 + core) * feat, feat)
     my_cols = pl.ds(pl.multiple_of(me_tp * feat, 128), feat)
-    send(psend1.at[0], precv1.at[0], ps_sem.at[0], pr_sem.at[segs], partner).wait_recv()
+    near_copy.wait_recv()
+
+    def near_total(rows):
+        return (
+            cur1[rows, my_cols].astype(F32) + own1[0, rows, :] + precv1[0, rows, :].astype(F32)
+        )
+
+    rows = pl.ds(head, DIRECT)
+    total = near_total(rows)
+    for k in range(1, n_x):
+        for n in range(2):
+            direct_copy(k, n).wait_recv()
+            total = total + drecv[k - 1, n].astype(F32)
+    out[rows, :] = total.astype(BF16)
     for g in range(len(groups)):
-        rows = groups[g]
-        total = cur1[rows, my_cols].astype(F32) + own1[0, rows, :] + precv1[0, rows, :].astype(F32)
+        rows = summed_rows[g]
+        total = near_total(rows)
         for k in range(1, n_x):
             chip_copy1(g, k).wait_recv()
             total = total + xrecv1[k - 1, rows, :].astype(F32)
         out[rows, :] = total.astype(BF16)
 
-    send(psend1, precv1, ps_sem.at[0], pr_sem.at[0], partner).wait_send()
+    near_copy.wait_send()
     for k in range(1, n_x):
         send(
-            xsend1.at[k - 1], xrecv1.at[k - 1], xs_sem.at[k - 1], xr1_sem.at[k - 1, 0], peer(k)
+            psend1.at[k, beyond], precv1.at[k, beyond], ps_sem.at[k], pr_sem.at[0], partner
+        ).wait_send()
+        send(
+            xsend1.at[k - 1, beyond],
+            xrecv1.at[k - 1, beyond],
+            xs_sem.at[k - 1],
+            xr1_sem.at[k - 1, 0],
+            peer(k),
+        ).wait_send()
+        send(
+            dsend.at[k - 1], drecv.at[k - 1], ds_sem.at[k - 1], dr_sem.at[k - 1, 0], peer(k)
         ).wait_send()
     end_halo(1)
 
@@ -643,12 +693,15 @@
         pltpu.VMEM((n_x, row_count, feat), F32),
         pltpu.VMEM((others, row_count, feat), BF16),
         pltpu.VMEM((others, row_count, feat), BF16),
+        pltpu.VMEM((others, 2, DIRECT, feat), BF16),
+        pltpu.VMEM((others, 2, DIRECT, feat), BF16),
         dma((10,)),
-        dma((1,)), dma((segs + 1 + (others - 1) * segs,)),
+        dma((n_x,)), dma((segs + 1 + (others - 1) * segs,)),
         dma((others,)), dma((others, segs + half_width // min(half_width, 512) - 1)),
         dma((segs,)),
         dma((1,)), dma((2 + segs,)),
         dma((others, segs)),
+        dma((others,)), dma((others, 2)),
     ]
     return pl.pallas_call(
         functools.partial(body, n_sp, n_tp),

time: 32 us -> 31.9 us (level)
  no operation moved by 1% of the time
where the time goes in v5:
time: 31.9 us; the launch traced here: 31.8 us
  Pallas kernels  31.1 us (97%)
  local copies, waits for them, and re-layouts  0.71 us (2%)
    pallas_call x1, Pallas kernels, local(): pl.pallas_call(functools.partial(body, n_sp, n_tp), out_shape=pltpu.VMEM(...  31.1 us
    unnamed x1, local copies, waits for them, and re-layouts  0.71 us

profile of v5, /device:TPU:19, one launch (start us, length us, event | category | flops | bytes accessed | tf_op | source)
XLA Modules:
  0.0 31.8 jit_solution(2331494428530941510)
XLA Ops:
  0.0 31.1 %shard_map.91 = bf16[256,512]{1,0:T(8,128)(2,1)S(1)} custom-call(bf16[256,2048]{1,0:T(8,128)(2,1)} %stream.1, f32[2,2048]{1,0:T(2,128)} %attn_gain_in.1, bf16[2,2048,512]{2,1,0:T(8,128)(2,1)} %w_query.1, bf16[2,2048,128]{2,1,0:T(8,128)(2,1)} %w_key.1, bf16[2,2048,128]{2,1,0:T(8,128)(2,1)} %w_value.1, bf16[2,512,2048]{2,1,0:T(8,128)(2,1)} %w_out.1, ...), custom_call_target="tpu_custom_call" | custom-call | tf_op jit(solution)/shard_map/pallas_call | solution.py:706
  31.1 0.7 %copy.11 = bf16[256,512]{1,0:T(8,128)(2,1)} copy(bf16[256,512]{1,0:T(8,128)(2,1)S(1)} %shard_map.91) | data formatting | bytes 524288

commit v6 on v5

--- a/solution.py
+++ b/solution.py
@@ -15,7 +15,7 @@
 SPAN = (LEFT + 1) * SEG
 LINE = 384
 LOG2E = 1.4426950408889634
-DIRECT = 16
+DIRECT = 32
 
 norm_eps = 1e-06
 masked_score = -1e30

time: 31.9 us -> 31.9 us (level)
  no operation moved by 1% of the time
where the time goes in v6:
time: 31.9 us; the launch traced here: 31.8 us
  Pallas kernels  31 us (97%)
  local copies, waits for them, and re-layouts  0.71 us (2%)
    pallas_call x1, Pallas kernels, local(): pl.pallas_call(functools.partial(body, n_sp, n_tp), out_shape=pltpu.VMEM(...  31 us
    unnamed x1, local copies, waits for them, and re-layouts  0.71 us

profile of v6, /device:TPU:19, one launch (start us, length us, event | category | flops | bytes accessed | tf_op | source)
XLA Modules:
  0.0 31.8 jit_solution(17016432753126424166)
XLA Ops:
  0.0 31.0 %shard_map.91 = bf16[256,512]{1,0:T(8,128)(2,1)S(1)} custom-call(bf16[256,2048]{1,0:T(8,128)(2,1)} %stream.1, f32[2,2048]{1,0:T(2,128)} %attn_gain_in.1, bf16[2,2048,512]{2,1,0:T(8,128)(2,1)} %w_query.1, bf16[2,2048,128]{2,1,0:T(8,128)(2,1)} %w_key.1, bf16[2,2048,128]{2,1,0:T(8,128)(2,1)} %w_value.1, bf16[2,512,2048]{2,1,0:T(8,128)(2,1)} %w_out.1, ...), custom_call_target="tpu_custom_call" | custom-call | tf_op jit(solution)/shard_map/pallas_call | solution.py:706
  31.1 0.7 %copy.11 = bf16[256,512]{1,0:T(8,128)(2,1)} copy(bf16[256,512]{1,0:T(8,128)(2,1)S(1)} %shard_map.91) | data formatting | bytes 524288
